TPU v7x, 32 devices: a whole 2x2x4 slice. The times are simulated.
32 devices in a mesh: sp: 8 (over z, y), dp: 4 (over x, core).
Axes of the slice: x: 2, y: 2, z: 4, core: 2. Of those that a mesh axis runs over, the one named last changes fastest.
Arguments:
- gated: bfloat16 [4, 1024, 3072], P('dp', 'sp'), may hold values from -6 to 6
- values_in: bfloat16 [4, 1024, 3072], P('dp', 'sp'), may hold values from -6 to 6
- upstream: bfloat16 [4, 1024, 3072], P('dp', 'sp'), may hold values from -6 to 6
- gain: float32 [3072], replicated, may hold values from 0.1 to 1.9
- shift: float32 [3072], replicated, may hold values from -3 to 3
- mix_w: bfloat16 [512, 4, 512], P('dp'), may hold values from -0.375 to 0.375
- mix_bias: float32 [4, 512], replicated, may hold values from 0.1 to 1.9
Outputs:
- grad_u: bfloat16 [4, 1024, 3072], P('dp', 'sp')
- grad_v: bfloat16 [4, 1024, 3072], P('dp', 'sp')
- grad_mix: float32 [512, 4, 512], P('dp')
- grad_bias: float32 [4, 512], replicated
- grad_gain: float32 [3072], replicated
- grad_shift: float32 [3072], replicated
All inputs are finite; a program needn't handle non-finite values.
Results may differ from a plain program's by a relative error of at most 0.014.
Values may be sent and summed in bfloat16 or wider, within the bound.
A program may use at most 64 MiB of HBM per device.

v0:
```python
import functools

import jax
import jax.numpy as jnp
from jax import lax
from jax.experimental import pallas as pl
from jax.experimental.pallas import tpu as pltpu
from jax.sharding import PartitionSpec as P

SEG = 64


EPS = 1e-05

CHUNK = 16


def kernel(
    dims,
    gated_in,
    values_hbm,
    upstream_in,
    gain,
    shift,
    mix_w,
    mix_bias,
    grad_u,
    grad_v,
    group_r,
    summed,
    gated,
    values,
    upstream,
    my_w,
    tok_g,
    tok_n,
    recv_g,
    recv_n,
    back_s,
    mixed_s,
    ret_b,
    ret_n,
    w_all,
    term_s,
    term_r,
    dp_sum,
    span_r,
    span_sum,
    acc_gain,
    acc_shift,
    vec_a,
    vec_b,
    vec_c,
    vec_s,
    bias_t,
    sq_send,
    sq_recv,
    dp_send,
    dp_recv,
    sn_send,
    sn_recv,
    in_sem,
):
    tok, width, groups, span, dp_count, spans = dims
    half = groups * width
    rows = span // dp_count
    me = lax.axis_index("sp")
    my_span, k = me // groups, me % groups
    d = lax.axis_index("dp")
    f32, bf16 = jnp.float32, jnp.bfloat16

    def sq_id(j):
        return {"sp": my_span * groups + j}

    def dp_id(j):
        return {"dp": j}

    def sn_id(j):
        return {"sp": j * groups + k}

    class Exchange:
        def __init__(self, src, dst, own, count, where, send, recv, slot):
            self.src, self.dst, self.own, self.count = src, dst, own, count
            self.where, self.send, self.recv, self.slot = where, send, recv, slot

        def copy(self, step, to):
            peer = lax.rem(self.own + step, self.count)
            landing = self.own if to else peer
            return pltpu.make_async_remote_copy(
                src_ref=self.src(peer),
                dst_ref=self.dst(landing),
                send_sem=self.send.at[self.slot, step],
                recv_sem=self.recv.at[self.slot, landing],
                device_id=self.where(peer),
                device_id_type=pl.DeviceIdType.MESH,
            )

        def start(self):
            for step in range(1, self.count):
                self.copy(step, True).start()

        def arrive(self):
            for step in range(1, self.count):
                self.copy(step, False).wait_recv()

        def leave(self):
            for step in range(1, self.count):
                self.copy(step, True).wait_send()

    def square(src, dst, slot):
        return Exchange(src, dst, k, groups, sq_id, sq_send, sq_recv, slot)

    def across(src, dst, slot):
        return Exchange(src, dst, d, dp_count, dp_id, dp_send, dp_recv, slot)

    def spanning(src, dst, slot):
        return Exchange(src, dst, my_span, spans, sn_id, sn_send, sn_recv, slot)

    def w_rows(j):
        return w_all.at[pl.ds(pl.multiple_of(j * rows, rows), rows)]

    go_w = across(lambda j: my_w, w_rows, 0)
    go_g = square(lambda j: tok_g.at[j], lambda j: recv_g.at[j], 0)
    go_n = square(lambda j: tok_n.at[j], lambda j: recv_n.at[j], 1)
    go_b = square(lambda j: back_s.at[j], lambda j: ret_b.at[j], 2)
    go_m = square(lambda j: mixed_s.at[j], lambda j: ret_n.at[j], 3)
    go_t = across(
        lambda j: term_s.at[pl.ds(pl.multiple_of(j * rows, rows), rows)],
        lambda j: term_r.at[j],
        1,
    )
    go_s = spanning(lambda j: dp_sum, lambda j: span_r.at[j], 0)
    go_q = square(lambda j: span_sum, lambda j: group_r.at[j], 4)
    go_va = across(lambda j: vec_s.at[0], lambda j: vec_a.at[j], 2)
    go_vb = square(lambda j: vec_s.at[1], lambda j: vec_b.at[j], 5)
    go_vc = spanning(lambda j: vec_s.at[2], lambda j: vec_c.at[j], 1)

    fetches = [
        pltpu.make_async_copy(src, dst, in_sem.at[i])
        for i, (src, dst) in enumerate(
            ((gated_in, gated), (upstream_in, upstream), (values_hbm, values))
        )
    ]
    for fetch in fetches:
        fetch.start()

    barrier = pltpu.get_barrier_semaphore()
    for own, count, where in ((k, groups, sq_id), (d, dp_count, dp_id), (my_span, spans, sn_id)):
        for step in range(1, count):
            pl.semaphore_signal(
                barrier,
                inc=1,
                device_id=where(lax.rem(own + step, count)),
                device_id_type=pl.DeviceIdType.MESH,
            )

    def piece(r):
        return pl.ds(pl.multiple_of(r * CHUNK, CHUNK), CHUNK)

    fetches[0].wait()
    fetches[1].wait()

    @pl.loop(0, tok // CHUNK)
    def _(r):
        at = piece(r)
        prod = (upstream[at, :].astype(f32) * gated[at, :].astype(f32)).astype(bf16)
        for g in range(groups):
            tok_g[g, at, :] = prod[:, g * width : (g + 1) * width]

    pl.semaphore_wait(barrier, groups + dp_count + spans - 3)
    go_g.start()

    @pl.loop(0, rows // CHUNK)
    def _(r):
        at = piece(r)
        whole = mix_w[at].astype(f32)
        rows_of = whole[:, 0, :]
        for g in range(1, groups):
            rows_of = jnp.where(k == g, whole[:, g, :], rows_of)
        my_w[at, :] = rows_of.astype(bf16)

    go_w.start()
    fetches[2].wait()

    def unit_of(at):
        raw = values[at, :].astype(f32)
        centred = raw - jnp.mean(raw, axis=-1, keepdims=True)
        inv_std = lax.rsqrt(jnp.mean(centred * centred, axis=-1, keepdims=True) + EPS)
        return centred * inv_std, inv_std

    @pl.loop(0, tok // CHUNK)
    def _(r):
        at = piece(r)
        unit, _inv = unit_of(at)
        normed = (unit * gain[...] + shift[...]).astype(bf16)
        for g in range(groups):
            tok_n[g, at, :] = normed[:, g * width : (g + 1) * width]

    go_n.start()
    w_rows(d)[...] = my_w[...]
    recv_g[k] = tok_g[k]
    recv_n[k] = tok_n[k]
    acc_gain[...] = jnp.zeros_like(acc_gain)
    acc_shift[...] = jnp.zeros_like(acc_shift)
    bias_t[...] = jnp.transpose(jnp.broadcast_to(mix_bias[pl.ds(k, 1), :], (128, span)))

    def allowed(first, count):
        t = first + lax.broadcasted_iota(jnp.int32, (count, span), 0)
        s = lax.broadcasted_iota(jnp.int32, (count, span), 1)
        return lax.div(t, SEG) >= lax.div(s, SEG)

    go_w.arrive()
    for j in range(groups):
        at = slice(j * tok, (j + 1) * tok)
        w_all[at, :] = jnp.where(allowed(j * tok, tok), w_all[at, :].astype(f32), 0.0).astype(bf16)

    go_g.arrive()
    for j in range(groups):
        block = lax.dot_general(
            w_all[:, j * tok : (j + 1) * tok],
            recv_g[...].reshape(span, width),
            (((0,), (0,)), ((), ())),
            preferred_element_type=f32,
        )
        back_s[j] = block.astype(bf16)
    go_b.start()
    ret_b[k] = back_s[k]

    go_n.arrive()
    for j in range(groups):
        block = lax.dot_general(
            recv_g[j],
            recv_n[...].reshape(span, width),
            (((1,), (1,)), ((), ())),
            preferred_element_type=f32,
        )
        term_s[j * tok : (j + 1) * tok, :] = jnp.where(allowed(j * tok, tok), block, 0.0).astype(bf16)
    go_t.start()
    term_r[d] = term_s[pl.ds(pl.multiple_of(d * rows, rows), rows), :]
    for j in range(groups):
        block = jnp.dot(
            w_all[j * tok : (j + 1) * tok, :],
            recv_n[...].reshape(span, width),
            preferred_element_type=f32,
        )
        bias = bias_t[j * tok : (j + 1) * tok, :]
        for c in range(width // 128):
            lanes = slice(c * 128, (c + 1) * 128)
            mixed_s[j, :, lanes] = (block[:, lanes] + bias).astype(bf16)
    go_m.start()
    ret_n[k] = mixed_s[k]

    bias_sum = lax.dot_general(
        jnp.ones((8, width), bf16),
        recv_g[...].reshape(span, width),
        (((1,), (1,)), ((), ())),
        preferred_element_type=f32,
    )[0:1]

    def total(ref, count):
        out = ref[0].astype(f32)
        for i in range(1, count):
            out = out + ref[i].astype(f32)
        return out

    go_t.arrive()
    dp_sum[...] = total(term_r, dp_count).astype(bf16)
    go_s.start()
    span_r[my_span] = dp_sum[...]

    go_b.arrive()

    @pl.loop(0, tok // CHUNK)
    def _(r):
        at = piece(r)
        unit, inv_std = unit_of(at)
        grad_normed = jnp.concatenate([ret_b[g, at, :] for g in range(groups)], axis=1).astype(f32)
        acc_gain[...] += grad_normed * unit
        acc_shift[...] += grad_normed
        scaled = grad_normed * gain[...]
        grad_v[at, :] = (
            inv_std
            * (
                scaled
                - jnp.mean(scaled, axis=-1, keepdims=True)
                - unit * jnp.mean(scaled * unit, axis=-1, keepdims=True)
            )
        ).astype(bf16)

    parts = half // span
    gain_sum = jnp.sum(acc_gain[...], axis=0, keepdims=True)
    shift_sum = jnp.sum(acc_shift[...], axis=0, keepdims=True)
    for i in range(parts):
        vec_s[0, i : i + 1, :] = gain_sum[:, i * span : (i + 1) * span]
        vec_s[0, parts + i : parts + i + 1, :] = shift_sum[:, i * span : (i + 1) * span]
    for g in range(groups):
        vec_s[0, 2 * parts + g : 2 * parts + g + 1, :] = jnp.where(k == g, bias_sum, 0.0)
    go_va.start()
    vec_a[d] = vec_s[0]

    go_va.arrive()
    vec_s[1] = total(vec_a, dp_count)
    go_vb.start()
    vec_b[k] = vec_s[1]

    go_s.arrive()
    span_sum[...] = total(span_r, spans).astype(bf16)
    go_q.start()
    group_r[k] = span_sum[...]

    go_vb.arrive()
    vec_s[2] = total(vec_b, groups)
    go_vc.start()
    vec_c[my_span] = vec_s[2]

    go_m.arrive()

    @pl.loop(0, tok // CHUNK)
    def _(r):
        at = piece(r)
        mixed = jnp.concatenate([ret_n[g, at, :] for g in range(groups)], axis=1).astype(f32)
        grad_u[at, :] = (upstream[at, :].astype(f32) * mixed).astype(bf16)

    go_vc.arrive()
    summed[...] = total(vec_c, spans)
    go_q.arrive()

    for go in (go_w, go_g, go_n, go_b, go_m, go_t, go_s, go_q, go_va, go_vb, go_vc):
        go.leave()


def finish(
    u_in, v_in, group_r, summed, grad_u, grad_v, grad_mix, grad_bias, grad_gain, grad_shift, sems
):
    copies = [
        pltpu.make_async_copy(u_in, grad_u, sems.at[0]),
        pltpu.make_async_copy(v_in, grad_v, sems.at[1]),
    ]
    for copy in copies:
        copy.start()
    groups, span = grad_bias.shape
    parts = grad_gain.shape[-1] // span
    for g in range(groups):
        grad_mix[:, g, :] = group_r[g].astype(jnp.float32)
    for i in range(parts):
        grad_gain[:, i * span : (i + 1) * span] = summed[i : i + 1, :]
        grad_shift[:, i * span : (i + 1) * span] = summed[parts + i : parts + i + 1, :]
    grad_bias[...] = summed[2 * parts : 2 * parts + groups, :]
    for copy in copies:
        copy.wait()


def per_device(gated, values_in, upstream, gain, shift, mix_w, mix_bias):
    dp_count = lax.axis_size("dp")
    sp_count = lax.axis_size("sp")
    tok, half = gated.shape[1:]
    rows, groups, span = mix_w.shape
    width = half // groups
    assert span == groups * tok
    spans = sp_count // groups
    vec_rows = 2 * (half // span) + groups
    f32, bf16 = jnp.float32, jnp.bfloat16
    block = pltpu.VMEM((groups, tok, width), bf16)
    hbm = pl.BlockSpec(memory_space=pltpu.HBM)
    scratch = (
        [pltpu.VMEM((tok, half), bf16)] * 3
        + [pltpu.VMEM((rows, span), bf16)]
        + [block] * 8
        + [
            pltpu.VMEM((span, span), bf16),
            pltpu.VMEM((span, span), bf16),
            pltpu.VMEM((dp_count, rows, span), bf16),
            pltpu.VMEM((rows, span), bf16),
            pltpu.VMEM((spans, rows, span), bf16),
            pltpu.VMEM((rows, span), bf16),
            pltpu.VMEM((CHUNK, half), f32),
            pltpu.VMEM((CHUNK, half), f32),
            pltpu.VMEM((dp_count, vec_rows, span), f32),
            pltpu.VMEM((groups, vec_rows, span), f32),
            pltpu.VMEM((spans, vec_rows, span), f32),
            pltpu.VMEM((3, vec_rows, span), f32),
            pltpu.VMEM((span, 128), f32),
        ]
        + [pltpu.SemaphoreType.DMA((6, groups))] * 2
        + [pltpu.SemaphoreType.DMA((3, dp_count))] * 2
        + [pltpu.SemaphoreType.DMA((2, spans))] * 2
        + [pltpu.SemaphoreType.DMA((3,))]
    )
    vmem = pl.BlockSpec(memory_space=pltpu.VMEM)
    out = pl.pallas_call(
        functools.partial(kernel, (tok, width, groups, span, dp_count, spans)),
        out_shape=(
            jax.ShapeDtypeStruct((tok, half), bf16),
            jax.ShapeDtypeStruct((tok, half), bf16),
            jax.ShapeDtypeStruct((groups, rows, span), bf16),
            jax.ShapeDtypeStruct((vec_rows, span), f32),
        ),
        in_specs=[hbm] * 3 + [vmem] * 4,
        out_specs=[vmem] * 4,
        scratch_shapes=scratch,
        compiler_params=pltpu.CompilerParams(
            collective_id=0, has_side_effects=True, vmem_limit_bytes=60 * 1024 * 1024
        ),
    )(
        gated[0],
        values_in[0],
        upstream[0],
        gain[None],
        shift[None],
        mix_w,
        mix_bias,
    )
    u, v, mix, bias, gain_g, shift_g = pl.pallas_call(
        finish,
        out_shape=(
            jax.ShapeDtypeStruct((tok, half), bf16),
            jax.ShapeDtypeStruct((tok, half), bf16),
            jax.ShapeDtypeStruct((rows, groups, span), f32),
            jax.ShapeDtypeStruct((groups, span), f32),
            jax.ShapeDtypeStruct((1, half), f32),
            jax.ShapeDtypeStruct((1, half), f32),
        ),
        in_specs=[vmem] * 4,
        out_specs=[hbm] * 2 + [vmem] * 4,
        scratch_shapes=[pltpu.SemaphoreType.DMA((2,))],
        compiler_params=pltpu.CompilerParams(vmem_limit_bytes=60 * 1024 * 1024),
    )(*out)
    return (u[None], v[None], mix, bias, gain_g[0], shift_g[0])


def solution(mesh):
    placed = (
        P("dp", "sp", None),
        P("dp", "sp", None),
        P("dp", "sp", None),
        P(),
        P(),
        P("dp", None, None),
        P(),
    )
    return jax.shard_map(
        per_device,
        mesh=mesh,
        in_specs=placed,
        out_specs=(P("dp", "sp", None), P("dp", "sp", None), P("dp", None, None), P(), P(), P()),
        check_vma=False,
    )
```

profile of v0, /device:TPU:0, one launch (start us, length us, event | category | flops | bytes accessed | tf_op | source)
XLA Modules:
  0.0 58.3 jit_solution(2520590516789577024)
XLA Ops:
  0.6 54.0 %shard_map.118 = (bf16[128,3072]{1,0:T(8,128)(2,1)}, bf16[128,3072]{1,0:T(8,128)(2,1)}, bf16[4,128,512]{2,1,0:T(8,128)(2,1)}, f32[16,512]{1,0:T(8,128)}) custom-call(bf16[128,3072]{1,0:T(8,128)(2,1)} %bitcast.9, bf16[128,3072]{1,0:T(8,128)(2,1)} %bitcast.10, bf16[128,3072]{1,0:T(8,128)(2,1)} %bitcast.11, f32[1,3072]{1,0:T(1,128)} %bitcast.12, ...), custom_call_target="tpu_custom_call" | custom-call | tf_op jit(solution)/shard_map/pallas_call | solution.py:390
  54.7 3.7 %shard_map.119 = (bf16[128,3072]{1,0:T(8,128)(2,1)}, bf16[128,3072]{1,0:T(8,128)(2,1)}, f32[128,4,512]{2,1,0:T(4,128)}, f32[4,512]{1,0:T(4,128)}, f32[1,3072]{1,0:T(1,128)}, /*index=5*/f32[1,3072]{1,0:T(1,128)}) custom-call(bf16[128,3072]{1,0:T(8,128)(2,1)} %get-tuple-element.16.u_in, bf16[128,3072]{1,0:T(8,128)(2,1)} %get-tuple-element.17.v_in, ...), custom_call_target="tpu_custom_call" | custom-call | tf_op jit(solution)/shard_map/pallas_call | solution.py:413
where the time goes:
time: 58.5 us; the launch traced here: 58.3 us
  Pallas kernels  57.7 us (99%)
  between operations  0.64 us (1%)
    pallas_call x1, Pallas kernels, per_device(): pl.pallas_call(functools.partial(kernel, (tok, width, groups, span, dp_co...  54 us
    pallas_call x1, Pallas kernels, per_device(): pl.pallas_call(finish, out_shape=(jax.ShapeDtypeStruct((tok, half), bf16)...  3.65 us

commit v1 on v0

v1 whole, which is shorter than its diff:
```python
import functools

import jax
import jax.numpy as jnp
from jax import lax
from jax.experimental import pallas as pl
from jax.experimental.pallas import tpu as pltpu
from jax.sharding import PartitionSpec as P

SEG = 64

EPS = 1e-05

CHUNK = 16

QUAD = 4


def nt(a, b):
    return lax.dot_general(a, b, (((1,), (1,)), ((), ())), preferred_element_type=jnp.float32)


def tn(a, b):
    return lax.dot_general(a, b, (((0,), (0,)), ((), ())), preferred_element_type=jnp.float32)


def nn(a, b):
    return jnp.dot(a, b, preferred_element_type=jnp.float32)


def kernel(
    dims,
    gated_in,
    values_in,
    upstream_in,
    gain,
    shift,
    mix_in,
    mix_bias,
    grad_u,
    grad_v,
    grad_mix,
    summed,
    gated,
    values,
    upstream,
    mix_w,
    unit,
    inv,
    nbuf,
    gbuf,
    w_send,
    w_block,
    stage_y,
    stage_z,
    recv_y,
    recv_z,
    own_part,
    back,
    sum_a,
    sum_b,
    acc_gain,
    acc_shift,
    term_w,
    term_n,
    red_w,
    red_n,
    dp_w,
    dp_n,
    span_w,
    span_n,
    all_w,
    all_n,
    vec_a,
    vec_b,
    vec_c,
    vec_s,
    bias_t,
    raw_sems,
    part_sems,
    dp_send,
    dp_recv,
    sn_send,
    sn_recv,
    sq_send,
    sq_recv,
    in_sem,
):
    tok, width, groups, span, dp_count, spans = dims
    half = groups * width
    rows = span // dp_count
    per_block = tok // rows
    hg = groups // 2
    me = lax.axis_index("sp")
    my_span, k = me // QUAD, lax.rem(me, QUAD)
    zb, yb = k // 2, lax.rem(k, 2)
    d = lax.axis_index("dp")
    t_own = d // per_block
    f32, bf16 = jnp.float32, jnp.bfloat16

    def sq_id(j):
        return {"sp": my_span * QUAD + j}

    def dp_id(j):
        return {"dp": j}

    def sn_id(j):
        return {"sp": j * QUAD + k}

    y_id = sq_id(k + 1 - 2 * yb)
    z_id = sq_id(k + 2 - 4 * zb)

    def remote(src, dst, send, recv, where):
        return pltpu.make_async_remote_copy(
            src_ref=src,
            dst_ref=dst,
            send_sem=send,
            recv_sem=recv,
            device_id=where,
            device_id_type=pl.DeviceIdType.MESH,
        )

    class Exchange:
        def __init__(self, src, dst, own, count, where, send, recv, slot, gives=None, takes=None):
            self.src, self.dst, self.own, self.count = src, dst, own, count
            self.where, self.send, self.recv, self.slot = where, send, recv, slot
            self.gives, self.takes = gives, takes

        def copy(self, step, to):
            peer = lax.rem(self.own + step, self.count)
            landing = self.own if to else peer
            return remote(
                self.src(peer) if to else self.dst(landing),
                self.dst(landing),
                self.send.at[self.slot, step],
                self.recv.at[self.slot, landing],
                self.where(peer),
            )

        def each(self, cond, act):
            for step in range(1, self.count):
                if cond is None:
                    act(step)
                else:
                    pl.when(cond(lax.rem(self.own + step, self.count)))(lambda: act(step))

        def start(self):
            self.each(self.gives, lambda step: self.copy(step, True).start())

        def arrive(self):
            self.each(self.takes, lambda step: self.copy(step, False).wait_recv())

        def leave(self):
            self.each(self.gives, lambda step: self.copy(step, True).wait_send())

    def square(src, dst, slot, gives=None, takes=None):
        return Exchange(src, dst, k, QUAD, sq_id, sq_send, sq_recv, slot, gives, takes)

    def across(src, dst, slot, gives=None, takes=None):
        return Exchange(src, dst, d, dp_count, dp_id, dp_send, dp_recv, slot, gives, takes)

    def spanning(src, dst, slot, gives=None, takes=None):
        return Exchange(src, dst, my_span, spans, sn_id, sn_send, sn_recv, slot, gives, takes)

    fetches = [
        pltpu.make_async_copy(src, dst, in_sem.at[i])
        for i, (src, dst) in enumerate(
            (
                (gated_in, gated),
                (upstream_in, upstream),
                (values_in, values),
                (mix_in, mix_w),
            )
        )
    ]
    for fetch in (fetches[2], fetches[0], fetches[1], fetches[3]):
        fetch.start()

    barrier = pltpu.get_barrier_semaphore()
    for own, count, where in (
        (k, QUAD, sq_id),
        (d, dp_count, dp_id),
        (my_span, spans, sn_id),
    ):
        for step in range(1, count):
            pl.semaphore_signal(
                barrier,
                inc=1,
                device_id=where(lax.rem(own + step, count)),
                device_id_type=pl.DeviceIdType.MESH,
            )

    def piece(r):
        return pl.ds(pl.multiple_of(r * CHUNK, CHUNK), CHUNK)

    def lanes_of(g):
        return slice(g * width, (g + 1) * width)

    def allowed(first_t, first_s, n_t, n_s):
        t = first_t + lax.broadcasted_iota(jnp.int32, (n_t, n_s), 0)
        s = first_s + lax.broadcasted_iota(jnp.int32, (n_t, n_s), 1)
        return lax.div(t, SEG) >= lax.div(s, SEG)

    def run(z):
        first = range(hg)
        second = range(hg, groups)
        wide = first if z == 0 else second
        narrow = second if z == 0 else first
        n_own = {g: yb if (z == 0 or g in first) else 1 for g in range(groups)}
        g_own = {g: yb if (z == 1 or g in second) else 0 for g in range(groups)}

        def makes_w(t):
            return (lax.rem(t, 2) == yb) if z == 0 else (t >= 2)

        def slot_w(t):
            return lax.div(t, 2) if z == 0 else t - 2

        def makes_n(t):
            return t == k

        def of(j):
            return j // per_block

        def part(j):
            return lax.rem(j, per_block)

        x_buf = nbuf if z == 0 else gbuf
        o_buf = gbuf if z == 0 else nbuf
        raw_y = {}
        for g in wide:
            raw_y[g] = x_buf
        y_send = {
            g: remote(
                x_buf.at[g, yb], x_buf.at[g, yb], raw_sems.at[0, g], raw_sems.at[1, g], y_id
            )
            for g in wide
        }
        y_take = {
            g: remote(
                x_buf.at[g, 1 - yb],
                x_buf.at[g, 1 - yb],
                raw_sems.at[0, g],
                raw_sems.at[1, g],
                y_id,
            )
            for g in wide
        }

        def narrow_y(buf, slot, g):
            return remote(
                buf.at[g, slot], buf.at[g, slot], raw_sems.at[0, g], raw_sems.at[1, g], y_id
            )

        z_buf = nbuf if z == 0 else gbuf
        z_own = n_own if z == 0 else g_own
        z_slot = 0 if z == 0 else 1
        z_send = {
            g: remote(
                z_buf.at[g, z_own[g]],
                z_buf.at[g, z_slot],
                raw_sems.at[2, g],
                raw_sems.at[3, g],
                z_id,
            )
            for g in narrow
        }
        z_take = {
            g: remote(
                o_buf.at[g, 1 - z_slot],
                o_buf.at[g, 1 - z_slot],
                raw_sems.at[2, g],
                raw_sems.at[3, g],
                z_id,
            )
            for g in wide
        }
        py = [
            remote(stage_y.at[i], recv_y.at[i], part_sems.at[0, i], part_sems.at[1, i], y_id)
            for i in range(hg)
        ]
        pz = [
            remote(stage_z.at[i], recv_z.at[i], part_sems.at[2, i], part_sems.at[3, i], z_id)
            for i in range(hg)
        ]

        def needs(h):
            return makes_w if h == z else ((lambda t: t < 2) if z == 0 else (lambda t: t >= 2))

        def slot_of(h, t):
            return slot_w(t) if h == z else (t if z == 0 else t - 2)

        def w_at(h, j):
            return w_block.at[slot_of(h, of(j)) * per_block + part(j), h * hg : (h + 1) * hg]

        go_mix = [
            across(
                lambda j, h=h: w_send.at[h * hg : (h + 1) * hg],
                lambda j, h=h: w_at(h, j),
                h,
                lambda j, h=h: needs(h)(t_own),
                lambda j, h=h: needs(h)(of(j)),
            )
            for h in range(2)
        ]
        go_tw = across(
            lambda j: term_w.at[slot_w(of(j)) * per_block + part(j)],
            lambda j: red_w.at[j],
            2,
            lambda j: makes_w(of(j)),
            lambda j: makes_w(t_own),
        )
        go_tn = across(
            lambda j: term_n.at[part(j)],
            lambda j: red_n.at[j],
            3,
            lambda j: makes_n(of(j)),
            lambda j: makes_n(t_own),
        )
        go_sw = spanning(
            lambda j: dp_w,
            lambda j: span_w.at[j],
            0,
            lambda j: makes_w(t_own),
            lambda j: makes_w(t_own),
        )
        go_sn = spanning(
            lambda j: dp_n,
            lambda j: span_n.at[j],
            1,
            lambda j: makes_n(t_own),
            lambda j: makes_n(t_own),
        )

        def peer_w(j):
            return ((j < 2) & (lax.rem(t_own, 2) == j)) | ((j >= 2) & (t_own >= 2))

        go_aw = square(
            lambda j: all_w.at[k],
            lambda j: all_w.at[j],
            0,
            lambda j: makes_w(t_own),
            peer_w,
        )
        go_an = square(
            lambda j: all_n.at[k],
            lambda j: all_n.at[j],
            1,
            lambda j: makes_n(t_own),
            lambda j: t_own == j,
        )
        go_va = across(lambda j: vec_s.at[0], lambda j: vec_a.at[j], 4)
        go_vb = square(lambda j: vec_s.at[1], lambda j: vec_b.at[j], 2)
        go_vc = spanning(lambda j: vec_s.at[2], lambda j: vec_c.at[j], 2)

        def make_normed():
            fetches[2].wait()

            @pl.loop(0, tok // CHUNK)
            def _(r):
                at = piece(r)
                raw = values[at, :].astype(f32)
                centred = raw - jnp.mean(raw, axis=-1, keepdims=True)
                inv_std = lax.rsqrt(jnp.mean(centred * centred, axis=-1, keepdims=True) + EPS)
                one = centred * inv_std
                unit[at, :] = one
                inv[at, :] = jnp.broadcast_to(inv_std, (CHUNK, 128))
                normed = (one * gain[...] + shift[...]).astype(bf16)
                for g in range(groups):
                    nbuf[g, n_own[g], at, :] = normed[:, lanes_of(g)]

        def make_cotangent():
            fetches[0].wait()
            fetches[1].wait()

            @pl.loop(0, tok // CHUNK)
            def _(r):
                at = piece(r)
                prod = (upstream[at, :].astype(f32) * gated[at, :].astype(f32)).astype(bf16)
                for g in range(groups):
                    gbuf[g, g_own[g], at, :] = prod[:, lanes_of(g)]

        def meet():
            pl.semaphore_wait(barrier, QUAD + dp_count + spans - 3)

        def narrow_n():
            @pl.when(yb == 0)
            def _():
                for g in narrow:
                    narrow_y(nbuf, 0, g).start()

        def narrow_g():
            @pl.when(yb == 1)
            def _():
                for g in narrow:
                    narrow_y(gbuf, 1, g).start()

        (make_normed if z == 0 else make_cotangent)()
        meet()
        for g, h in zip(wide, narrow):
            y_send[g].start()
            z_send[h].start()
        (narrow_n if z == 0 else narrow_g)()
        (make_cotangent if z == 0 else make_normed)()
        (narrow_g if z == 0 else narrow_n)()

        @pl.when(yb == 0)
        def _():
            for g in narrow:
                nbuf[g, 1] = jnp.zeros((tok, width), bf16)

        @pl.when(yb == 1)
        def _():
            for g in narrow:
                gbuf[g, 0] = jnp.zeros((tok, width), bf16)

        fetches[3].wait()

        @pl.loop(0, rows // CHUNK)
        def _(r):
            at = piece(r)
            for c in range(2):
                for h in range(2):
                    if z == 0:
                        col = c
                    elif h == 0:
                        col = 2 + c
                    else:
                        col = yb + 2 * c
                    start = col * tok
                    if not isinstance(start, int):
                        start = pl.multiple_of(start, tok)
                    block = mix_w[at, :, pl.ds(start, tok)].astype(f32)
                    keep = allowed(d * rows + r * CHUNK, col * tok, CHUNK, tok)
                    for g in range(h * hg, (h + 1) * hg):
                        w_send[g, at, c * tok : (c + 1) * tok] = jnp.where(
                            keep, block[:, g, :], 0.0
                        ).astype(bf16)

        for h in (z, 1 - z):
            go_mix[h].start()

            @pl.when(needs(h)(t_own))
            def _():
                w_at(h, d)[...] = w_send[h * hg : (h + 1) * hg]

        own_bias = mix_bias[:, 0:tok]
        for b in range(1, QUAD):
            own_bias = jnp.where(k == b, mix_bias[:, b * tok : (b + 1) * tok], own_bias)
        for g in range(groups):
            bias_t[g] = jnp.transpose(jnp.broadcast_to(own_bias[g : g + 1], (128, tok)))
        acc_gain[...] = jnp.zeros_like(acc_gain)
        acc_shift[...] = jnp.zeros_like(acc_shift)
        sum_a[...] = jnp.zeros_like(sum_a)
        sum_b[...] = jnp.zeros_like(sum_b)
        grad_mix[...] = jnp.zeros_like(grad_mix)
        parts = half // span
        for g in range(groups):
            bias_sum = nt(jnp.ones((8, width), bf16), gbuf[g, g_own[g]])[0:1]
            at = 2 * parts + g
            for b in range(QUAD):
                vec_s[0, at : at + 1, b * tok : (b + 1) * tok] = jnp.where(k == b, bias_sum, 0.0)

        def give_u(g, mixed):
            for c in range(width // 128):
                lanes = slice(c * 128, (c + 1) * 128)
                at = slice(g * width + c * 128, g * width + (c + 1) * 128)
                whole = (mixed[:, lanes] + bias_t[g]).astype(bf16).astype(f32)
                grad_u[:, at] = (upstream[:, at].astype(f32) * whole).astype(bf16)

        def give_back(g, total):
            back[g] = total.astype(bf16)

            @pl.loop(0, tok // CHUNK)
            def _(r):
                at = piece(r)
                grad_normed = back[g, at, :].astype(f32)
                one = unit[at, lanes_of(g)]
                prod = grad_normed * one
                acc_gain[:, lanes_of(g)] += prod[0:8] + prod[8:16]
                acc_shift[:, lanes_of(g)] += grad_normed[0:8] + grad_normed[8:16]
                scaled = grad_normed * gain[:, lanes_of(g)]
                prod = scaled * one
                a, b = scaled[:, 0:128], prod[:, 0:128]
                for c in range(1, width // 128):
                    a = a + scaled[:, c * 128 : (c + 1) * 128]
                    b = b + prod[:, c * 128 : (c + 1) * 128]
                sum_a[at, :] += a
                sum_b[at, :] += b

        def give_v():
            @pl.loop(0, tok // CHUNK)
            def _(r):
                at = piece(r)
                mean_a = jnp.sum(sum_a[at, :], axis=-1, keepdims=True) / half
                mean_b = jnp.sum(sum_b[at, :], axis=-1, keepdims=True) / half
                inv_std = inv[at, :][:, 0:1]
                for g in range(groups):
                    scaled = back[g, at, :].astype(f32) * gain[:, lanes_of(g)]
                    grad_v[at, lanes_of(g)] = (
                        inv_std * (scaled - mean_a - unit[at, lanes_of(g)] * mean_b)
                    ).astype(bf16)

        def own_cols(g, block):
            at = pl.ds(pl.multiple_of(block * tok, tok), tok)
            return w_block[:, g, :, at].reshape(2 * tok, tok)

        def own_rows(g, block):
            return w_block[pl.ds(block * per_block, per_block), g].reshape(tok, 2 * tok)

        def pair(buf, g):
            return buf[g].reshape(2 * tok, width)

        go_mix[z].arrive()
        for i, g in enumerate(wide):
            y_take[g].wait_recv()
            if z == 0:
                both = nn(w_block[:, g].reshape(2 * tok, 2 * tok), pair(nbuf, g))
                stage_z[i] = both[tok:].astype(bf16)
                pz[i].start()
                give_u(g, both[:tok])
            else:
                both = tn(w_block[:, g].reshape(2 * tok, 2 * tok), pair(gbuf, g))
                stage_z[i] = both[:tok].astype(bf16)
                pz[i].start()
                give_back(g, both[tok:])
        for i, g in enumerate(wide):
            z_take[g].wait_recv()
            if z == 0:
                stage_y[i] = tn(own_cols(g, 1 - yb), pair(gbuf, g)).astype(bf16)
                py[i].start()
                own_part[i] = tn(own_cols(g, yb), pair(gbuf, g))
            else:
                stage_y[i] = nn(own_rows(g, 1 - yb), pair(nbuf, g)).astype(bf16)
                py[i].start()
                own_part[i] = nn(own_rows(g, yb), pair(nbuf, g))

        def keep_of(row, col):
            return allowed(row * tok, col * tok, tok, tok)

        for i, g in enumerate(wide):
            block = nt(pair(gbuf, g), pair(nbuf, g))
            for a in range(2):
                for b in range(2):
                    if z == 0:
                        keep = keep_of(yb + 2 * a, b)
                    else:
                        keep = keep_of(2 + a, yb + 2 * b)
                    at, of_s = slice(a * tok, (a + 1) * tok), slice(b * tok, (b + 1) * tok)
                    kept = jnp.where(keep, block[at, of_s], 0.0).astype(bf16)
                    for p in range(per_block):
                        term_w[a * per_block + p, i, :, of_s] = kept[p * rows : (p + 1) * rows]
        go_tw.start()

        go_mix[1 - z].arrive()
        for i, g in enumerate(narrow):

            @pl.when(yb == 1)
            def _():
                narrow_y(nbuf, 0, g).wait_recv()

            @pl.when(yb == 0)
            def _():
                narrow_y(gbuf, 1, g).wait_recv()

            block = nt(gbuf[g, g_own[g]], pair(nbuf, g))
            for b in range(2):
                of_s = slice(b * tok, (b + 1) * tok)
                keep = keep_of(k, b if z == 0 else 2 + b)
                kept = jnp.where(keep, block[:, of_s], 0.0).astype(bf16)
                for p in range(per_block):
                    term_n[p, i, :, of_s] = kept[p * rows : (p + 1) * rows]
        go_tn.start()

        def total(ref, count):
            out = ref[0].astype(f32)
            for i in range(1, count):
                out = out + ref[i].astype(f32)
            return out

        @pl.when(makes_w(t_own))
        def _():
            red_w[d] = term_w[slot_w(t_own) * per_block + part(d)]
            go_tw.arrive()
            dp_w[...] = total(red_w, dp_count).astype(bf16)
            span_w[my_span] = dp_w[...]

        go_sw.start()

        for i, g in enumerate(narrow):
            if z == 0:
                give_u(g, nn(own_rows(g, yb), pair(nbuf, g)))
            else:
                own_n = tn(own_cols(g, yb), pair(gbuf, g))
                give_back(g, own_n)
        for i, g in enumerate(narrow):
            pz_take = pz[i]
            pz_take.wait_recv()
            if z == 0:
                own_n = tn(own_cols(g, yb), pair(gbuf, g))
                give_back(g, recv_z[i].astype(f32) + own_n)
            else:
                give_u(g, recv_z[i].astype(f32) + nn(own_rows(g, yb), pair(nbuf, g)))

        @pl.when(makes_n(t_own))
        def _():
            red_n[d] = term_n[part(d)]
            go_tn.arrive()
            dp_n[...] = total(red_n, dp_count).astype(bf16)
            span_n[my_span] = dp_n[...]

        go_sn.start()

        @pl.when(makes_w(t_own))
        def _():
            go_sw.arrive()
            all_w[k] = total(span_w, spans).astype(bf16)

        go_aw.start()

        def send_vectors():
            gain_sum = jnp.sum(acc_gain[...], axis=0, keepdims=True)
            shift_sum = jnp.sum(acc_shift[...], axis=0, keepdims=True)
            for i in range(parts):
                vec_s[0, i : i + 1, :] = gain_sum[:, i * span : (i + 1) * span]
                vec_s[0, parts + i : parts + i + 1, :] = shift_sum[:, i * span : (i + 1) * span]
            go_va.start()
            vec_a[d] = vec_s[0]

        if z == 1:
            send_vectors()
            give_v()

        @pl.when(makes_n(t_own))
        def _():
            go_sn.arrive()
            all_n[k] = total(span_n, spans).astype(bf16)

        go_an.start()

        for i, g in enumerate(wide):
            py[i].wait_recv()
            whole = own_part[i] + recv_y[i].astype(f32)
            if z == 0:
                give_back(g, whole)
            else:
                give_u(g, whole)
        if z == 0:
            send_vectors()
            give_v()

        go_va.arrive()
        vec_s[1] = total(vec_a, dp_count)
        go_vb.start()
        vec_b[k] = vec_s[1]

        go_aw.arrive()
        go_an.arrive()

        def put(g, first, block):
            grad_mix[:, g, first * tok : first * tok + block.shape[1]] = block.astype(f32)

        for i in range(hg):
            put(i, 0, all_w[lax.rem(t_own, 2), i])

        @pl.when(t_own >= 2)
        def _():
            for i in range(hg):
                put(i, 2, all_n[t_own, i])
                for b in range(2):
                    put(hg + i, b, all_w[2 + b, i][:, :tok])
                    put(hg + i, b + 2, all_w[2 + b, i][:, tok:])

        @pl.when(t_own < 2)
        def _():
            for i in range(hg):
                put(hg + i, 0, all_n[t_own, i])

        go_vb.arrive()
        vec_s[2] = total(vec_b, QUAD)
        go_vc.start()
        vec_c[my_span] = vec_s[2]
        go_vc.arrive()
        summed[...] = total(vec_c, spans)

        for g in wide:
            y_send[g].wait_send()
        for g in narrow:
            z_send[g].wait_send()

            @pl.when(yb == 0)
            def _():
                narrow_y(nbuf, 0, g).wait_send()

            @pl.when(yb == 1)
            def _():
                narrow_y(gbuf, 1, g).wait_send()

        for i in range(hg):
            py[i].wait_send()
            pz[i].wait_send()
        for go in go_mix + [go_tw, go_tn, go_sw, go_sn, go_aw, go_an, go_va, go_vb, go_vc]:
            go.leave()

    for z in range(2):
        pl.when(zb == z)(functools.partial(run, z))


def finish(
    u_in, v_in, mix_in, summed, grad_u, grad_v, grad_mix, grad_bias, grad_gain, grad_shift, sems
):
    copies = [
        pltpu.make_async_copy(src, dst, sems.at[i])
        for i, (src, dst) in enumerate(((u_in, grad_u), (v_in, grad_v), (mix_in, grad_mix)))
    ]
    for copy in copies:
        copy.start()
    groups, span = grad_bias.shape
    parts = grad_gain.shape[-1] // span
    for i in range(parts):
        grad_gain[:, i * span : (i + 1) * span] = summed[i : i + 1, :]
        grad_shift[:, i * span : (i + 1) * span] = summed[parts + i : parts + i + 1, :]
    grad_bias[...] = summed[2 * parts : 2 * parts + groups, :]
    for copy in copies:
        copy.wait()


def per_device(gated, values_in, upstream, gain, shift, mix_w, mix_bias):
    dp_count = lax.axis_size("dp")
    sp_count = lax.axis_size("sp")
    tok, half = gated.shape[1:]
    rows, groups, span = mix_w.shape
    width = half // groups
    assert span == QUAD * tok and groups % 2 == 0 and tok % rows == 0
    spans = sp_count // QUAD
    hg = groups // 2
    vec_rows = 2 * (half // span) + groups
    f32, bf16 = jnp.float32, jnp.bfloat16
    hbm = pl.BlockSpec(memory_space=pltpu.HBM)
    vmem = pl.BlockSpec(memory_space=pltpu.VMEM)
    dma = pltpu.SemaphoreType.DMA
    term = (hg, rows, 2 * tok)
    scratch = (
        [pltpu.VMEM((tok, half), bf16)] * 3
        + [
            pltpu.VMEM((rows, groups, span), bf16),
            pltpu.VMEM((tok, half), f32),
            pltpu.VMEM((tok, 128), f32),
            pltpu.VMEM((groups, 2, tok, width), bf16),
            pltpu.VMEM((groups, 2, tok, width), bf16),
            pltpu.VMEM((groups, rows, 2 * tok), bf16),
            pltpu.VMEM((2 * (tok // rows), groups, rows, 2 * tok), bf16),
        ]
        + [pltpu.VMEM((hg, tok, width), bf16)] * 4
        + [
            pltpu.VMEM((hg, tok, width), f32),
            pltpu.VMEM((groups, tok, width), bf16),
            pltpu.VMEM((tok, 128), f32),
            pltpu.VMEM((tok, 128), f32),
            pltpu.VMEM((8, half), f32),
            pltpu.VMEM((8, half), f32),
            pltpu.VMEM((2 * (tok // rows),) + term, bf16),
            pltpu.VMEM((tok // rows,) + term, bf16),
            pltpu.VMEM((dp_count,) + term, bf16),
            pltpu.VMEM((dp_count,) + term, bf16),
            pltpu.VMEM(term, bf16),
            pltpu.VMEM(term, bf16),
            pltpu.VMEM((spans,) + term, bf16),
            pltpu.VMEM((spans,) + term, bf16),
            pltpu.VMEM((QUAD,) + term, bf16),
            pltpu.VMEM((QUAD,) + term, bf16),
            pltpu.VMEM((dp_count, vec_rows, span), f32),
            pltpu.VMEM((QUAD, vec_rows, span), f32),
            pltpu.VMEM((spans, vec_rows, span), f32),
            pltpu.VMEM((3, vec_rows, span), f32),
            pltpu.VMEM((groups, tok, 128), f32),
        ]
        + [dma((4, groups)), dma((4, hg))]
        + [dma((5, dp_count))] * 2
        + [dma((3, spans))] * 2
        + [dma((3, QUAD))] * 2
        + [dma((4,))]
    )
    out = pl.pallas_call(
        functools.partial(kernel, (tok, width, groups, span, dp_count, spans)),
        out_shape=(
            jax.ShapeDtypeStruct((tok, half), bf16),
            jax.ShapeDtypeStruct((tok, half), bf16),
            jax.ShapeDtypeStruct((rows, groups, span), f32),
            jax.ShapeDtypeStruct((vec_rows, span), f32),
        ),
        in_specs=[hbm] * 3 + [vmem] * 2 + [hbm, vmem],
        out_specs=[vmem] * 4,
        scratch_shapes=scratch,
        compiler_params=pltpu.CompilerParams(
            collective_id=0, has_side_effects=True, vmem_limit_bytes=60 * 1024 * 1024
        ),
    )(
        gated[0],
        values_in[0],
        upstream[0],
        gain[None],
        shift[None],
        mix_w,
        mix_bias,
    )
    u, v, mix, bias, gain_g, shift_g = pl.pallas_call(
        finish,
        out_shape=(
            jax.ShapeDtypeStruct((tok, half), bf16),
            jax.ShapeDtypeStruct((tok, half), bf16),
            jax.ShapeDtypeStruct((rows, groups, span), f32),
            jax.ShapeDtypeStruct((groups, span), f32),
            jax.ShapeDtypeStruct((1, half), f32),
            jax.ShapeDtypeStruct((1, half), f32),
        ),
        in_specs=[vmem] * 4,
        out_specs=[hbm] * 3 + [vmem] * 3,
        scratch_shapes=[pltpu.SemaphoreType.DMA((3,))],
        compiler_params=pltpu.CompilerParams(vmem_limit_bytes=60 * 1024 * 1024),
    )(*out)
    return (u[None], v[None], mix, bias, gain_g[0], shift_g[0])


def solution(mesh):
    placed = (
        P("dp", "sp", None),
        P("dp", "sp", None),
        P("dp", "sp", None),
        P(),
        P(),
        P("dp", None, None),
        P(),
    )
    return jax.shard_map(
        per_device,
        mesh=mesh,
        in_specs=placed,
        out_specs=(P("dp", "sp", None), P("dp", "sp", None), P("dp", None, None), P(), P(), P()),
        check_vma=False,
    )
```

time: 58.5 us -> 54.1 us (0.925)
  the two profiles are of different devices: /device:TPU:0 before, /device:TPU:6 now
where the time goes in v1:
time: 54.1 us; the launch traced here: 53.9 us
  Pallas kernels  53.2 us (98%)
  between operations  0.64 us (1%)
    pallas_call x1, Pallas kernels, per_device(): pl.pallas_call(functools.partial(kernel, (tok, width, groups, span, dp_co...  49.4 us
    pallas_call x1, Pallas kernels, per_device(): pl.pallas_call(finish, out_shape=(jax.ShapeDtypeStruct((tok, half), bf16)...  3.83 us

profile of v1, /device:TPU:6, one launch (start us, length us, event | category | flops | bytes accessed | tf_op | source)
XLA Modules:
  0.0 53.9 jit_solution(7550040194286301460)
XLA Ops:
  0.6 49.4 %shard_map.118 = (bf16[128,3072]{1,0:T(8,128)(2,1)}, bf16[128,3072]{1,0:T(8,128)(2,1)}, f32[128,4,512]{2,1,0:T(4,128)}, f32[16,512]{1,0:T(8,128)}) custom-call(bf16[128,3072]{1,0:T(8,128)(2,1)} %bitcast.9, bf16[128,3072]{1,0:T(8,128)(2,1)} %bitcast.10, bf16[128,3072]{1,0:T(8,128)(2,1)} %bitcast.11, f32[1,3072]{1,0:T(1,128)} %bitcast.12, f32[1,3072]{1,0:T(1,128)} %bitcast.13, ...), custom_call_target="tpu_custom_call" | custom-call | tf_op jit(solution)/shard_map/pallas_call | solution.py:783
  50.1 3.8 %shard_map.119 = (bf16[128,3072]{1,0:T(8,128)(2,1)}, bf16[128,3072]{1,0:T(8,128)(2,1)}, f32[128,4,512]{2,1,0:T(4,128)}, f32[4,512]{1,0:T(4,128)}, f32[1,3072]{1,0:T(1,128)}, /*index=5*/f32[1,3072]{1,0:T(1,128)}) custom-call(bf16[128,3072]{1,0:T(8,128)(2,1)} %get-tuple-element.16.u_in, bf16[128,3072]{1,0:T(8,128)(2,1)} %get-tuple-element.17.v_in, ...), custom_call_target="tpu_custom_call" | custom-call | tf_op jit(solution)/shard_map/pallas_call | solution.py:806

commit v2 on v1

--- a/solution.py
+++ b/solution.py
@@ -33,10 +33,10 @@
     gated_in,
     values_in,
     upstream_in,
-    gain,
-    shift,
+    gain_in,
+    shift_in,
     mix_in,
-    mix_bias,
+    bias_in,
     grad_u,
     grad_v,
     grad_mix,
@@ -45,6 +45,9 @@
     values,
     upstream,
     mix_w,
+    gain,
+    shift,
+    mix_bias,
     unit,
     inv,
     nbuf,
@@ -62,24 +65,35 @@
     acc_gain,
     acc_shift,
     term_w,
-    term_n,
+    term_d,
+    term_l,
     red_w,
-    red_n,
+    red_d,
+    red_l,
     dp_w,
-    dp_n,
+    dp_d,
+    dp_l,
     span_w,
-    span_n,
+    span_d,
+    span_l,
     all_w,
-    all_n,
-    vec_a,
-    vec_b,
-    vec_c,
-    vec_s,
+    all_d,
+    all_l,
+    late_s,
+    late_a,
+    late_b,
+    early_s,
+    early_a,
+    early_b,
+    early_c,
     bias_t,
     raw_sems,
     part_sems,
+    z_sems,
     dp_send,
-    dp_recv,
+    mix_recv,
+    red_recv,
+    vec_sems,
     sn_send,
     sn_recv,
     sq_send,
@@ -107,6 +121,9 @@
     def sn_id(j):
         return {"sp": j * QUAD + k}
 
+    def sp_id(j):
+        return {"sp": j}
+
     y_id = sq_id(k + 1 - 2 * yb)
     z_id = sq_id(k + 2 - 4 * zb)
 
@@ -121,19 +138,22 @@
         )
 
     class Exchange:
-        def __init__(self, src, dst, own, count, where, send, recv, slot, gives=None, takes=None):
+        def __init__(
+            self, src, dst, own, count, where, send, recv, gives=None, takes=None, bulk=None
+        ):
             self.src, self.dst, self.own, self.count = src, dst, own, count
-            self.where, self.send, self.recv, self.slot = where, send, recv, slot
-            self.gives, self.takes = gives, takes
+            self.where, self.send, self.recv = where, send, recv
+            self.gives, self.takes, self.bulk = gives, takes, bulk
 
         def copy(self, step, to):
             peer = lax.rem(self.own + step, self.count)
             landing = self.own if to else peer
+            by = step if to else self.count - step
             return remote(
                 self.src(peer) if to else self.dst(landing),
                 self.dst(landing),
-                self.send.at[self.slot, step],
-                self.recv.at[self.slot, landing],
+                self.send(step - 1),
+                self.recv(by - 1),
                 self.where(peer),
             )
 
@@ -144,23 +164,42 @@
                 else:
                     pl.when(cond(lax.rem(self.own + step, self.count)))(lambda: act(step))
 
+        def all_of_it(self):
+            where = self.where(lax.rem(self.own + 1, self.count))
+            return remote(self.bulk, self.bulk, self.send(0), self.recv(0), where)
+
         def start(self):
             self.each(self.gives, lambda step: self.copy(step, True).start())
 
         def arrive(self):
-            self.each(self.takes, lambda step: self.copy(step, False).wait_recv())
+            if self.bulk is None:
+                self.each(self.takes, lambda step: self.copy(step, False).wait_recv())
+            elif self.takes is None:
+                self.all_of_it().wait_recv()
+            else:
+                pl.when(self.takes(self.own))(lambda: self.all_of_it().wait_recv())
 
         def leave(self):
-            self.each(self.gives, lambda step: self.copy(step, True).wait_send())
-
-    def square(src, dst, slot, gives=None, takes=None):
-        return Exchange(src, dst, k, QUAD, sq_id, sq_send, sq_recv, slot, gives, takes)
-
-    def across(src, dst, slot, gives=None, takes=None):
-        return Exchange(src, dst, d, dp_count, dp_id, dp_send, dp_recv, slot, gives, takes)
+            if self.bulk is None or self.gives is not None:
+                self.each(self.gives, lambda step: self.copy(step, True).wait_send())
+            else:
+                self.all_of_it().wait_send()
+
+    def across(src, dst, send, recv, gives=None, takes=None, bulk=None):
+        return Exchange(src, dst, d, dp_count, dp_id, send, recv, gives, takes, bulk)
 
     def spanning(src, dst, slot, gives=None, takes=None):
-        return Exchange(src, dst, my_span, spans, sn_id, sn_send, sn_recv, slot, gives, takes)
+        return Exchange(
+            src,
+            dst,
+            my_span,
+            spans,
+            sn_id,
+            lambda step: sn_send.at[slot, step],
+            lambda step: sn_recv.at[slot, step],
+            gives,
+            takes,
+        )
 
     fetches = [
         pltpu.make_async_copy(src, dst, in_sem.at[i])
@@ -170,18 +209,17 @@
                 (upstream_in, upstream),
                 (values_in, values),
                 (mix_in, mix_w),
+                (gain_in, gain),
+                (shift_in, shift),
+                (bias_in, mix_bias),
             )
         )
     ]
-    for fetch in (fetches[2], fetches[0], fetches[1], fetches[3]):
+    for fetch in (*fetches[4:], fetches[2], fetches[0], fetches[1], fetches[3]):
         fetch.start()
 
     barrier = pltpu.get_barrier_semaphore()
-    for own, count, where in (
-        (k, QUAD, sq_id),
-        (d, dp_count, dp_id),
-        (my_span, spans, sn_id),
-    ):
+    for own, count, where in ((me, spans * QUAD, sp_id), (d, dp_count, dp_id)):
         for step in range(1, count):
             pl.semaphore_signal(
                 barrier,
@@ -258,21 +296,21 @@
             g: remote(
                 z_buf.at[g, z_own[g]],
                 z_buf.at[g, z_slot],
-                raw_sems.at[2, g],
-                raw_sems.at[3, g],
+                z_sems.at[0, i],
+                z_sems.at[1, i],
                 z_id,
             )
-            for g in narrow
+            for i, g in enumerate(narrow)
         }
         z_take = {
             g: remote(
                 o_buf.at[g, 1 - z_slot],
                 o_buf.at[g, 1 - z_slot],
-                raw_sems.at[2, g],
-                raw_sems.at[3, g],
+                z_sems.at[0, i],
+                z_sems.at[1, i],
                 z_id,
             )
-            for g in wide
+            for i, g in enumerate(wide)
         }
         py = [
             remote(stage_y.at[i], recv_y.at[i], part_sems.at[0, i], part_sems.at[1, i], y_id)
@@ -296,66 +334,213 @@
             across(
                 lambda j, h=h: w_send.at[h * hg : (h + 1) * hg],
                 lambda j, h=h: w_at(h, j),
-                h,
+                lambda step, h=h: dp_send.at[h, step],
+                lambda step, h=h: mix_recv.at[h, step],
                 lambda j, h=h: needs(h)(t_own),
                 lambda j, h=h: needs(h)(of(j)),
             )
             for h in range(2)
         ]
-        go_tw = across(
-            lambda j: term_w.at[slot_w(of(j)) * per_block + part(j)],
-            lambda j: red_w.at[j],
-            2,
-            lambda j: makes_w(of(j)),
-            lambda j: makes_w(t_own),
-        )
-        go_tn = across(
-            lambda j: term_n.at[part(j)],
-            lambda j: red_n.at[j],
-            3,
-            lambda j: makes_n(of(j)),
-            lambda j: makes_n(t_own),
-        )
-        go_sw = spanning(
-            lambda j: dp_w,
-            lambda j: span_w.at[j],
-            0,
-            lambda j: makes_w(t_own),
-            lambda j: makes_w(t_own),
-        )
-        go_sn = spanning(
-            lambda j: dp_n,
-            lambda j: span_n.at[j],
-            1,
-            lambda j: makes_n(t_own),
-            lambda j: makes_n(t_own),
-        )
+        def makes_l(t):
+            return (t == k) & (yb == 1)
 
         def peer_w(j):
             return ((j < 2) & (lax.rem(t_own, 2) == j)) | ((j >= 2) & (t_own >= 2))
 
-        go_aw = square(
-            lambda j: all_w.at[k],
-            lambda j: all_w.at[j],
-            0,
-            lambda j: makes_w(t_own),
-            peer_w,
+        def peer_d(j):
+            return t_own == j
+
+        def peer_l(j):
+            return (t_own == j) & (lax.rem(j, 2) == 1)
+
+        class Reduction:
+            def __init__(self, makes, peer, source, refs, slot):
+                red, dp_sum, over, every, bulk = refs
+                self.makes, self.refs, self.source = makes, refs, source
+                self.to_dp = across(
+                    source,
+                    lambda j: red(j),
+                    lambda step: dp_send.at[2 + slot, step],
+                    lambda step: red_recv.at[slot],
+                    lambda j: makes(of(j)),
+                    lambda j: makes(t_own),
+                    bulk,
+                )
+                self.to_span = spanning(
+                    lambda j: dp_sum,
+                    lambda j: over(j),
+                    slot,
+                    lambda j: makes(t_own),
+                    lambda j: makes(t_own),
+                )
+                self.peer = peer
+                row, column = k + 1 - 2 * yb, k + 2 - 4 * zb
+
+                def copy(piece, at, where):
+                    return remote(
+                        every(piece),
+                        every(piece),
+                        sq_send.at[slot, at],
+                        sq_recv.at[slot, at],
+                        where,
+                    )
+
+                self.own_z, self.own_y = copy(k, 0, z_id), copy(k, 1, y_id)
+                self.take_z, self.take_y = copy(column, 0, z_id), copy(row, 1, y_id)
+                self.relay_z = copy(row, 2, z_id)
+                self.take_relay = copy(3 - k, 2, z_id)
+                self.row, self.column = row, column
+
+            def start(self):
+                self.to_dp.start()
+
+            def over_spans(self):
+                red, dp_sum, over, every, _bulk = self.refs
+
+                @pl.when(self.makes(t_own))
+                def _():
+                    red(d)[...] = self.source(d)[...]
+                    self.to_dp.arrive()
+                    dp_sum[...] = total(red, dp_count).astype(bf16)
+                    self.to_span.start()
+                    over(my_span)[...] = dp_sum[...]
+
+            def pass_round(self):
+                red, dp_sum, over, every, _bulk = self.refs
+
+                @pl.when(self.makes(t_own))
+                def _():
+                    self.to_span.arrive()
+                    every(k)[...] = total(over, spans).astype(bf16)
+                    self.own_z.start()
+                    self.own_y.start()
+
+            def relay(self):
+                @pl.when(self.peer(self.row))
+                def _():
+                    self.take_y.wait_recv()
+                    self.relay_z.start()
+
+            def arrive(self):
+                pl.when(self.peer(self.column))(lambda: self.take_z.wait_recv())
+                pl.when(self.peer(3 - k))(lambda: self.take_relay.wait_recv())
+
+            def leave(self):
+                self.to_dp.leave()
+                self.to_span.leave()
+
+                @pl.when(self.makes(t_own))
+                def _():
+                    self.own_z.wait_send()
+                    self.own_y.wait_send()
+
+                pl.when(self.peer(self.row))(lambda: self.relay_z.wait_send())
+
+        def total(at, count):
+            out = at(0)[...].astype(f32)
+            for i in range(1, count):
+                out = out + at(i)[...].astype(f32)
+            return out
+
+        terms_w = [
+            Reduction(
+                makes_w,
+                peer_w,
+                lambda j, i=i: term_w.at[slot_w(of(j)) * per_block + part(j), i],
+                (
+                    lambda j, i=i: red_w.at[i, j],
+                    dp_w.at[i],
+                    lambda j, i=i: span_w.at[j, i],
+                    lambda j, i=i: all_w.at[j, i],
+                    red_w.at[i, : dp_count - 1],
+                ),
+                i,
+            )
+            for i in range(hg)
+        ]
+        terms_d = Reduction(
+            makes_n,
+            peer_d,
+            lambda j: term_d.at[part(j)],
+            (
+                lambda j: red_d.at[j],
+                dp_d,
+                lambda j: span_d.at[j],
+                lambda j: all_d.at[j],
+                red_d.at[: dp_count - 1],
+            ),
+            hg,
         )
-        go_an = square(
-            lambda j: all_n.at[k],
-            lambda j: all_n.at[j],
-            1,
-            lambda j: makes_n(t_own),
-            lambda j: t_own == j,
+        terms_l = Reduction(
+            makes_l,
+            peer_l,
+            lambda j: term_l.at[part(j)],
+            (
+                lambda j: red_l.at[j],
+                dp_l,
+                lambda j: span_l.at[j],
+                lambda j: all_l.at[j],
+                red_l.at[: dp_count - 1],
+            ),
+            hg + 1,
         )
-        go_va = across(lambda j: vec_s.at[0], lambda j: vec_a.at[j], 4)
-        go_vb = square(lambda j: vec_s.at[1], lambda j: vec_b.at[j], 2)
-        go_vc = spanning(lambda j: vec_s.at[2], lambda j: vec_c.at[j], 2)
+
+        def vec(at):
+            return lambda step: vec_sems.at[at]
+
+        late_go = (
+            across(
+                lambda j: late_s.at[0],
+                lambda j: late_a.at[j],
+                vec(0),
+                vec(1),
+                bulk=late_a.at[: dp_count - 1],
+            ),
+            Exchange(
+                lambda j: late_s.at[1],
+                lambda j: late_b.at[j],
+                me,
+                spans * QUAD,
+                sp_id,
+                vec(2),
+                vec(3),
+                bulk=late_b.at[: spans * QUAD - 1],
+            ),
+        )
+        early_go = (
+            across(
+                lambda j: early_s.at[0],
+                lambda j: early_a.at[j],
+                vec(4),
+                vec(5),
+                bulk=early_a.at[: dp_count - 1],
+            ),
+            Exchange(
+                lambda j: early_s.at[1],
+                lambda j: early_c.at[j],
+                me // 2,
+                spans * QUAD // 2,
+                lambda j: {"sp": 2 * j + lax.rem(me, 2)},
+                vec(6),
+                vec(7),
+                bulk=early_c.at[: spans * QUAD // 2 - 1],
+            ),
+            Exchange(
+                lambda j: early_s.at[2],
+                lambda j: early_b.at[j],
+                lax.rem(me, 2),
+                2,
+                lambda j: {"sp": me - lax.rem(me, 2) + j},
+                vec(8),
+                vec(9),
+            ),
+        )
 
         def make_normed():
-            fetches[2].wait()
-
-            @pl.loop(0, tok // CHUNK)
+            for fetch in (fetches[4], fetches[5], fetches[2]):
+                fetch.wait()
+
+            @pl.loop(0, tok // CHUNK, unroll=4)
             def _(r):
                 at = piece(r)
                 raw = values[at, :].astype(f32)
@@ -380,7 +565,7 @@
                     gbuf[g, g_own[g], at, :] = prod[:, lanes_of(g)]
 
         def meet():
-            pl.semaphore_wait(barrier, QUAD + dp_count + spans - 3)
+            pl.semaphore_wait(barrier, spans * QUAD + dp_count - 2)
 
         def narrow_n():
             @pl.when(yb == 0)
@@ -443,6 +628,14 @@
             def _():
                 w_at(h, d)[...] = w_send[h * hg : (h + 1) * hg]
 
+        for i, g in enumerate(narrow):
+            block = nt(gbuf[g, g_own[g]], nbuf[g, n_own[g]])
+            kept = jnp.where(allowed(0, 0, tok, tok), block, 0.0).astype(bf16)
+            for p in range(per_block):
+                term_d[p, i] = kept[p * rows : (p + 1) * rows]
+        terms_d.start()
+
+        fetches[6].wait()
         own_bias = mix_bias[:, 0:tok]
         for b in range(1, QUAD):
             own_bias = jnp.where(k == b, mix_bias[:, b * tok : (b + 1) * tok], own_bias)
@@ -453,12 +646,15 @@
         sum_a[...] = jnp.zeros_like(sum_a)
         sum_b[...] = jnp.zeros_like(sum_b)
         grad_mix[...] = jnp.zeros_like(grad_mix)
-        parts = half // span
+        lines = hg * width // 128
+        per_span = span // 128
         for g in range(groups):
             bias_sum = nt(jnp.ones((8, width), bf16), gbuf[g, g_own[g]])[0:1]
-            at = 2 * parts + g
             for b in range(QUAD):
-                vec_s[0, at : at + 1, b * tok : (b + 1) * tok] = jnp.where(k == b, bias_sum, 0.0)
+                shown = jnp.where(k == b, bias_sum, 0.0)
+                for c in range(tok // 128):
+                    at = 2 * lines + g * per_span + b * (tok // 128) + c
+                    early_s[0, at : at + 1, :] = shown[:, c * 128 : (c + 1) * 128]
 
         def give_u(g, mixed):
             for c in range(width // 128):
@@ -510,6 +706,52 @@
         def pair(buf, g):
             return buf[g].reshape(2 * tok, width)
 
+        def keep_of(row, col):
+            return allowed(row * tok, col * tok, tok, tok)
+
+        def gather_sums(h, out):
+            first = h * hg * width
+            for ref, line in ((acc_gain, 0), (acc_shift, lines)):
+                whole = jnp.sum(ref[:, first : first + hg * width], axis=0, keepdims=True)
+                for i in range(lines):
+                    out[0, line + i : line + i + 1, :] = whole[:, i * 128 : (i + 1) * 128]
+
+        def send_early():
+            gather_sums(1, early_s)
+            early_go[0].start()
+            early_a[d] = early_s[0]
+
+        def spread_early():
+            early_go[0].arrive()
+            early_s[1] = total(lambda j: early_a.at[j], dp_count)
+            early_go[1].start()
+            early_c[me // 2] = early_s[1]
+
+        def respread_early():
+            early_go[1].arrive()
+            early_s[2] = total(lambda j: early_c.at[j], spans * QUAD // 2)
+            early_go[2].start()
+            early_b[lax.rem(me, 2)] = early_s[2]
+
+        def send_late():
+            gather_sums(0, late_s)
+            late_go[0].start()
+            late_a[d] = late_s[0]
+
+        def spread_late():
+            late_go[0].arrive()
+            late_s[1] = total(lambda j: late_a.at[j], dp_count)
+            late_go[1].start()
+            late_b[me] = late_s[1]
+
+        def take_early():
+            early_go[2].arrive()
+            summed[2 * lines :, :] = total(lambda j: early_b.at[j], 2)
+
+        def take_late():
+            late_go[1].arrive()
+            summed[: 2 * lines, :] = total(lambda j: late_b.at[j], spans * QUAD)
+
         go_mix[z].arrive()
         for i, g in enumerate(wide):
             y_take[g].wait_recv()
@@ -523,21 +765,13 @@
                 stage_z[i] = both[:tok].astype(bf16)
                 pz[i].start()
                 give_back(g, both[tok:])
-        for i, g in enumerate(wide):
             z_take[g].wait_recv()
             if z == 0:
                 stage_y[i] = tn(own_cols(g, 1 - yb), pair(gbuf, g)).astype(bf16)
-                py[i].start()
-                own_part[i] = tn(own_cols(g, yb), pair(gbuf, g))
             else:
                 stage_y[i] = nn(own_rows(g, 1 - yb), pair(nbuf, g)).astype(bf16)
+            if z == 0 or i < hg - 1:
                 py[i].start()
-                own_part[i] = nn(own_rows(g, yb), pair(nbuf, g))
-
-        def keep_of(row, col):
-            return allowed(row * tok, col * tok, tok, tok)
-
-        for i, g in enumerate(wide):
             block = nt(pair(gbuf, g), pair(nbuf, g))
             for a in range(2):
                 for b in range(2):
@@ -549,95 +783,63 @@
                     kept = jnp.where(keep, block[at, of_s], 0.0).astype(bf16)
                     for p in range(per_block):
                         term_w[a * per_block + p, i, :, of_s] = kept[p * rows : (p + 1) * rows]
-        go_tw.start()
+            terms_w[i].start()
+            if z == 0:
+                own_part[i] = tn(own_cols(g, yb), pair(gbuf, g))
+            else:
+                own_part[i] = nn(own_rows(g, yb), pair(nbuf, g))
 
         go_mix[1 - z].arrive()
+        terms_d.over_spans()
         for i, g in enumerate(narrow):
+            terms_w[i].over_spans()
 
             @pl.when(yb == 1)
             def _():
                 narrow_y(nbuf, 0, g).wait_recv()
+                block = nt(gbuf[g, g_own[g]], nbuf[g, 0]).astype(bf16)
+                for p in range(per_block):
+                    term_l[p, i] = block[p * rows : (p + 1) * rows]
 
             @pl.when(yb == 0)
             def _():
                 narrow_y(gbuf, 1, g).wait_recv()
 
-            block = nt(gbuf[g, g_own[g]], pair(nbuf, g))
-            for b in range(2):
-                of_s = slice(b * tok, (b + 1) * tok)
-                keep = keep_of(k, b if z == 0 else 2 + b)
-                kept = jnp.where(keep, block[:, of_s], 0.0).astype(bf16)
-                for p in range(per_block):
-                    term_n[p, i, :, of_s] = kept[p * rows : (p + 1) * rows]
-        go_tn.start()
-
-        def total(ref, count):
-            out = ref[0].astype(f32)
-            for i in range(1, count):
-                out = out + ref[i].astype(f32)
-            return out
-
-        @pl.when(makes_w(t_own))
-        def _():
-            red_w[d] = term_w[slot_w(t_own) * per_block + part(d)]
-            go_tw.arrive()
-            dp_w[...] = total(red_w, dp_count).astype(bf16)
-            span_w[my_span] = dp_w[...]
-
-        go_sw.start()
-
-        for i, g in enumerate(narrow):
+            if i == hg - 1:
+                terms_l.start()
             if z == 0:
                 give_u(g, nn(own_rows(g, yb), pair(nbuf, g)))
+            pz[i].wait_recv()
+            if z == 0:
+                give_back(g, recv_z[i].astype(f32) + tn(own_cols(g, yb), pair(gbuf, g)))
             else:
-                own_n = tn(own_cols(g, yb), pair(gbuf, g))
-                give_back(g, own_n)
-        for i, g in enumerate(narrow):
-            pz_take = pz[i]
-            pz_take.wait_recv()
-            if z == 0:
-                own_n = tn(own_cols(g, yb), pair(gbuf, g))
-                give_back(g, recv_z[i].astype(f32) + own_n)
-            else:
+                give_back(g, tn(own_cols(g, yb), pair(gbuf, g)))
                 give_u(g, recv_z[i].astype(f32) + nn(own_rows(g, yb), pair(nbuf, g)))
 
-        @pl.when(makes_n(t_own))
-        def _():
-            red_n[d] = term_n[part(d)]
-            go_tn.arrive()
-            dp_n[...] = total(red_n, dp_count).astype(bf16)
-            span_n[my_span] = dp_n[...]
-
-        go_sn.start()
-
-        @pl.when(makes_w(t_own))
-        def _():
-            go_sw.arrive()
-            all_w[k] = total(span_w, spans).astype(bf16)
-
-        go_aw.start()
-
-        def send_vectors():
-            gain_sum = jnp.sum(acc_gain[...], axis=0, keepdims=True)
-            shift_sum = jnp.sum(acc_shift[...], axis=0, keepdims=True)
-            for i in range(parts):
-                vec_s[0, i : i + 1, :] = gain_sum[:, i * span : (i + 1) * span]
-                vec_s[0, parts + i : parts + i + 1, :] = shift_sum[:, i * span : (i + 1) * span]
-            go_va.start()
-            vec_a[d] = vec_s[0]
-
+        send_early()
         if z == 1:
-            send_vectors()
+            send_late()
+        terms_d.pass_round()
+        for term in terms_w:
+            term.pass_round()
+        if z == 1:
+            py[hg - 1].start()
+        if z == 1:
             give_v()
-
-        @pl.when(makes_n(t_own))
-        def _():
-            go_sn.arrive()
-            all_n[k] = total(span_n, spans).astype(bf16)
-
-        go_an.start()
+        spread_early()
+        if z == 1:
+            spread_late()
+        terms_l.over_spans()
+
+        def relay_terms():
+            for term in (terms_d, *terms_w):
+                term.relay()
 
         for i, g in enumerate(wide):
+            if z == 1 and i == hg - 1:
+                relay_terms()
+                respread_early()
+                terms_l.pass_round()
             py[i].wait_recv()
             whole = own_part[i] + recv_y[i].astype(f32)
             if z == 0:
@@ -645,42 +847,15 @@
             else:
                 give_u(g, whole)
         if z == 0:
-            send_vectors()
+            send_late()
+            respread_early()
+            spread_late()
+            terms_l.pass_round()
+            relay_terms()
             give_v()
-
-        go_va.arrive()
-        vec_s[1] = total(vec_a, dp_count)
-        go_vb.start()
-        vec_b[k] = vec_s[1]
-
-        go_aw.arrive()
-        go_an.arrive()
 
         def put(g, first, block):
             grad_mix[:, g, first * tok : first * tok + block.shape[1]] = block.astype(f32)
-
-        for i in range(hg):
-            put(i, 0, all_w[lax.rem(t_own, 2), i])
-
-        @pl.when(t_own >= 2)
-        def _():
-            for i in range(hg):
-                put(i, 2, all_n[t_own, i])
-                for b in range(2):
-                    put(hg + i, b, all_w[2 + b, i][:, :tok])
-                    put(hg + i, b + 2, all_w[2 + b, i][:, tok:])
-
-        @pl.when(t_own < 2)
-        def _():
-            for i in range(hg):
-                put(hg + i, 0, all_n[t_own, i])
-
-        go_vb.arrive()
-        vec_s[2] = total(vec_b, QUAD)
-        go_vc.start()
-        vec_c[my_span] = vec_s[2]
-        go_vc.arrive()
-        summed[...] = total(vec_c, spans)
 
         for g in wide:
             y_send[g].wait_send()
@@ -698,8 +873,50 @@
         for i in range(hg):
             py[i].wait_send()
             pz[i].wait_send()
-        for go in go_mix + [go_tw, go_tn, go_sw, go_sn, go_aw, go_an, go_va, go_vb, go_vc]:
+        for go in (*go_mix, late_go[0], early_go[0]):
             go.leave()
+
+        terms_d.arrive()
+        for t in range(QUAD):
+
+            @pl.when(t_own == t)
+            def _():
+                for i in range(hg):
+                    put(i if t >= 2 else hg + i, t, all_d[t, i])
+
+        terms_d.leave()
+        for i, term in enumerate(terms_w):
+            term.arrive()
+            put(i, 0, all_w[lax.rem(t_own, 2), i])
+
+            @pl.when(t_own >= 2)
+            def _():
+                for b in range(2):
+                    put(hg + i, b, all_w[2 + b, i][:, :tok])
+
+            for t in range(2, QUAD):
+
+                @pl.when(t_own == t)
+                def _():
+                    for b in range(t - 1):
+                        put(hg + i, b + 2, all_w[2 + b, i][:, tok:])
+
+            term.leave()
+        terms_l.relay()
+        terms_l.arrive()
+        for t in range(1, QUAD, 2):
+
+            @pl.when(t_own == t)
+            def _():
+                for i in range(hg):
+                    put(i if t >= 2 else hg + i, t - 1, all_l[t, i])
+
+        terms_l.leave()
+        take_early()
+        for go in early_go[1:]:
+            go.leave()
+        take_late()
+        late_go[1].leave()
 
     for z in range(2):
         pl.when(zb == z)(functools.partial(run, z))
@@ -715,11 +932,18 @@
     for copy in copies:
         copy.start()
     groups, span = grad_bias.shape
-    parts = grad_gain.shape[-1] // span
-    for i in range(parts):
-        grad_gain[:, i * span : (i + 1) * span] = summed[i : i + 1, :]
-        grad_shift[:, i * span : (i + 1) * span] = summed[parts + i : parts + i + 1, :]
-    grad_bias[...] = summed[2 * parts : 2 * parts + groups, :]
+    lines = grad_gain.shape[-1] // 2 // 128
+    per_span = span // 128
+    for h in range(2):
+        for i in range(lines):
+            to = slice((h * lines + i) * 128, (h * lines + i + 1) * 128)
+            at = 2 * h * lines + i
+            grad_gain[:, to] = summed[at : at + 1, :]
+            grad_shift[:, to] = summed[lines + at : lines + at + 1, :]
+    for g in range(groups):
+        for c in range(per_span):
+            at = 4 * lines + g * per_span + c
+            grad_bias[g : g + 1, c * 128 : (c + 1) * 128] = summed[at : at + 1, :]
     for copy in copies:
         copy.wait()
 
@@ -733,16 +957,21 @@
     assert span == QUAD * tok and groups % 2 == 0 and tok % rows == 0
     spans = sp_count // QUAD
     hg = groups // 2
-    vec_rows = 2 * (half // span) + groups
     f32, bf16 = jnp.float32, jnp.bfloat16
     hbm = pl.BlockSpec(memory_space=pltpu.HBM)
     vmem = pl.BlockSpec(memory_space=pltpu.VMEM)
     dma = pltpu.SemaphoreType.DMA
-    term = (hg, rows, 2 * tok)
+    term, slim = (hg, rows, 2 * tok), (hg, rows, tok)
+    late_rows = half // 128
+    early_rows = late_rows + groups * span // 128
+    assert half % 256 == 0 and tok % 128 == 0
     scratch = (
         [pltpu.VMEM((tok, half), bf16)] * 3
         + [
             pltpu.VMEM((rows, groups, span), bf16),
+            pltpu.VMEM((1, half), f32),
+            pltpu.VMEM((1, half), f32),
+            pltpu.VMEM((groups, span), f32),
             pltpu.VMEM((tok, half), f32),
             pltpu.VMEM((tok, 128), f32),
             pltpu.VMEM((groups, 2, tok, width), bf16),
@@ -759,26 +988,29 @@
             pltpu.VMEM((8, half), f32),
             pltpu.VMEM((8, half), f32),
             pltpu.VMEM((2 * (tok // rows),) + term, bf16),
-            pltpu.VMEM((tok // rows,) + term, bf16),
-            pltpu.VMEM((dp_count,) + term, bf16),
-            pltpu.VMEM((dp_count,) + term, bf16),
-            pltpu.VMEM(term, bf16),
-            pltpu.VMEM(term, bf16),
-            pltpu.VMEM((spans,) + term, bf16),
-            pltpu.VMEM((spans,) + term, bf16),
-            pltpu.VMEM((QUAD,) + term, bf16),
-            pltpu.VMEM((QUAD,) + term, bf16),
-            pltpu.VMEM((dp_count, vec_rows, span), f32),
-            pltpu.VMEM((QUAD, vec_rows, span), f32),
-            pltpu.VMEM((spans, vec_rows, span), f32),
-            pltpu.VMEM((3, vec_rows, span), f32),
+            pltpu.VMEM((tok // rows,) + slim, bf16),
+            pltpu.VMEM((tok // rows,) + slim, bf16),
+        ]
+        + [pltpu.VMEM((hg, dp_count, rows, 2 * tok), bf16)]
+        + [pltpu.VMEM((dp_count,) + shape, bf16) for shape in (slim, slim)]
+        + [pltpu.VMEM(shape, bf16) for shape in (term, slim, slim)]
+        + [pltpu.VMEM((spans,) + shape, bf16) for shape in (term, slim, slim)]
+        + [pltpu.VMEM((QUAD,) + shape, bf16) for shape in (term, slim, slim)]
+        + [
+            pltpu.VMEM((2, late_rows, 128), f32),
+            pltpu.VMEM((dp_count, late_rows, 128), f32),
+            pltpu.VMEM((sp_count, late_rows, 128), f32),
+            pltpu.VMEM((3, early_rows, 128), f32),
+            pltpu.VMEM((dp_count, early_rows, 128), f32),
+            pltpu.VMEM((2, early_rows, 128), f32),
+            pltpu.VMEM((sp_count // 2, early_rows, 128), f32),
             pltpu.VMEM((groups, tok, 128), f32),
         ]
-        + [dma((4, groups)), dma((4, hg))]
-        + [dma((5, dp_count))] * 2
-        + [dma((3, spans))] * 2
-        + [dma((3, QUAD))] * 2
-        + [dma((4,))]
+        + [dma((2, groups)), dma((4, hg)), dma((2, hg))]
+        + [dma((4 + hg, dp_count - 1)), dma((2, dp_count - 1)), dma((2 + hg,)), dma((10,))]
+        + [dma((2 + hg, spans - 1))] * 2
+        + [dma((2 + hg, 3))] * 2
+        + [dma((7,))]
     )
     out = pl.pallas_call(
         functools.partial(kernel, (tok, width, groups, span, dp_count, spans)),
@@ -786,22 +1018,27 @@
             jax.ShapeDtypeStruct((tok, half), bf16),
             jax.ShapeDtypeStruct((tok, half), bf16),
             jax.ShapeDtypeStruct((rows, groups, span), f32),
-            jax.ShapeDtypeStruct((vec_rows, span), f32),
+            jax.ShapeDtypeStruct((late_rows + early_rows, 128), f32),
         ),
-        in_specs=[hbm] * 3 + [vmem] * 2 + [hbm, vmem],
+        in_specs=[hbm] * 7,
         out_specs=[vmem] * 4,
         scratch_shapes=scratch,
         compiler_params=pltpu.CompilerParams(
-            collective_id=0, has_side_effects=True, vmem_limit_bytes=60 * 1024 * 1024
+            collective_id=0, has_side_effects=True, vmem_limit_bytes=36 * 1024 * 1024
         ),
     )(
-        gated[0],
-        values_in[0],
-        upstream[0],
-        gain[None],
-        shift[None],
-        mix_w,
-        mix_bias,
+        *(
+            pltpu.with_memory_space_constraint(x, pltpu.HBM)
+            for x in (
+                gated[0],
+                values_in[0],
+                upstream[0],
+                gain[None],
+                shift[None],
+                mix_w,
+                mix_bias,
+            )
+        )
     )
     u, v, mix, bias, gain_g, shift_g = pl.pallas_call(
         finish,
@@ -816,7 +1053,7 @@
         in_specs=[vmem] * 4,
         out_specs=[hbm] * 3 + [vmem] * 3,
         scratch_shapes=[pltpu.SemaphoreType.DMA((3,))],
-        compiler_params=pltpu.CompilerParams(vmem_limit_bytes=60 * 1024 * 1024),
+        compiler_params=pltpu.CompilerParams(vmem_limit_bytes=36 * 1024 * 1024),
     )(*out)
     return (u[None], v[None], mix, bias, gain_g[0], shift_g[0])
 

time: 54.1 us -> 46.2 us (0.85)
  the two profiles are of different devices: /device:TPU:6 before, /device:TPU:3 now
where the time goes in v2:
time: 46.2 us; the launch traced here: 46 us
  Pallas kernels  45.4 us (98%)
  between operations  0.64 us (1%)
    pallas_call x1, Pallas kernels, per_device(): pl.pallas_call(functools.partial(kernel, (tok, width, groups, span, dp_co...  43.2 us
    pallas_call x1, Pallas kernels, per_device(): pl.pallas_call(finish, out_shape=(jax.ShapeDtypeStruct((tok, half), bf16)...  2.12 us

profile of v2, /device:TPU:3, one launch (start us, length us, event | category | flops | bytes accessed | tf_op | source)
XLA Modules:
  0.0 46.0 jit_solution(6736820371049176311)
XLA Ops:
  0.6 43.2 %shard_map.118 = (bf16[128,3072]{1,0:T(8,128)(2,1)S(1)}, bf16[128,3072]{1,0:T(8,128)(2,1)S(1)}, f32[128,4,512]{2,1,0:T(4,128)S(1)}, f32[64,128]{1,0:T(8,128)S(1)}) custom-call(bf16[128,3072]{1,0:T(8,128)(2,1)} %bitcast.9, bf16[128,3072]{1,0:T(8,128)(2,1)} %bitcast.10, bf16[128,3072]{1,0:T(8,128)(2,1)} %bitcast.11, f32[1,3072]{1,0:T(1,128)} %bitcast.12, ...), custom_call_target="tpu_custom_call" | custom-call | tf_op jit(solution)/shard_map/pallas_call | solution.py:1015
  43.9 2.1 %shard_map.119 = (bf16[128,3072]{1,0:T(8,128)(2,1)}, bf16[128,3072]{1,0:T(8,128)(2,1)}, f32[128,4,512]{2,1,0:T(4,128)}, f32[4,512]{1,0:T(4,128)}, f32[1,3072]{1,0:T(1,128)}, /*index=5*/f32[1,3072]{1,0:T(1,128)}) custom-call(bf16[128,3072]{1,0:T(8,128)(2,1)S(1)} %get-tuple-element.16.u_in, bf16[128,3072]{1,0:T(8,128)(2,1)S(1)} %get-tuple-element.17.v_in, ...), custom_call_target="tpu_custom_call" | custom-call | tf_op jit(solution)/shard_map/pallas_call | solution.py:1043

commit v3 on v2

--- a/solution.py
+++ b/solution.py
@@ -40,7 +40,9 @@
     grad_u,
     grad_v,
     grad_mix,
-    summed,
+    grad_gain,
+    grad_shift,
+    grad_bias,
     gated,
     values,
     upstream,
@@ -215,8 +217,12 @@
             )
         )
     ]
-    for fetch in (*fetches[4:], fetches[2], fetches[0], fetches[1], fetches[3]):
-        fetch.start()
+    for z, order in ((0, (4, 5, 2, 0, 1, 3, 6)), (1, (0, 1, 2, 4, 5, 3, 6))):
+
+        @pl.when(zb == z)
+        def _():
+            for i in order:
+                fetches[i].start()
 
     barrier = pltpu.get_barrier_semaphore()
     for own, count, where in ((me, spans * QUAD, sp_id), (d, dp_count, dp_id)):
@@ -354,7 +360,7 @@
             return (t_own == j) & (lax.rem(j, 2) == 1)
 
         class Reduction:
-            def __init__(self, makes, peer, source, refs, slot):
+            def __init__(self, makes, peer, source, refs, slot, passes):
                 red, dp_sum, over, every, bulk = refs
                 self.makes, self.refs, self.source = makes, refs, source
                 self.to_dp = across(
@@ -385,11 +391,24 @@
                         where,
                     )
 
-                self.own_z, self.own_y = copy(k, 0, z_id), copy(k, 1, y_id)
-                self.take_z, self.take_y = copy(column, 0, z_id), copy(row, 1, y_id)
-                self.relay_z = copy(row, 2, z_id)
-                self.take_relay = copy(3 - k, 2, z_id)
-                self.row, self.column = row, column
+                self.own_z = lambda: copy(k, 0, z_id)
+                self.own_y = lambda: copy(k, 1, y_id)
+                self.take_z = lambda: copy(column, 0, z_id)
+                self.take_y = lambda: copy(row, 1, y_id)
+                self.relays = {
+                    "column": lambda: remote(
+                        every(column),
+                        every(column),
+                        sq_send.at[slot, 2],
+                        sq_recv.at[slot, 2],
+                        y_id,
+                    ),
+                    "row": lambda: remote(
+                        every(row), every(row), sq_send.at[slot, 3], sq_recv.at[slot, 2], z_id
+                    ),
+                }
+                self.take_relay = lambda: copy(3 - k, 2, z_id)
+                self.row, self.column, self.passes = row, column, passes
 
             def start(self):
                 self.to_dp.start()
@@ -412,18 +431,27 @@
                 def _():
                     self.to_span.arrive()
                     every(k)[...] = total(over, spans).astype(bf16)
-                    self.own_z.start()
-                    self.own_y.start()
-
-            def relay(self):
+                    self.own_z().start()
+                    self.own_y().start()
+
+            def relay_column(self):
+                @pl.when(self.peer(self.column))
+                def _():
+                    self.take_z().wait_recv()
+                    self.relays["column"]().start()
+
+            def relay_row(self):
                 @pl.when(self.peer(self.row))
                 def _():
-                    self.take_y.wait_recv()
-                    self.relay_z.start()
+                    self.take_y().wait_recv()
+                    self.relays["row"]().start()
 
             def arrive(self):
-                pl.when(self.peer(self.column))(lambda: self.take_z.wait_recv())
-                pl.when(self.peer(3 - k))(lambda: self.take_relay.wait_recv())
+                if "column" not in self.passes:
+                    pl.when(self.peer(self.column))(lambda: self.take_z().wait_recv())
+                if "row" not in self.passes:
+                    pl.when(self.peer(self.row))(lambda: self.take_y().wait_recv())
+                pl.when(self.peer(3 - k))(lambda: self.take_relay().wait_recv())
 
             def leave(self):
                 self.to_dp.leave()
@@ -431,10 +459,12 @@
 
                 @pl.when(self.makes(t_own))
                 def _():
-                    self.own_z.wait_send()
-                    self.own_y.wait_send()
-
-                pl.when(self.peer(self.row))(lambda: self.relay_z.wait_send())
+                    self.own_z().wait_send()
+                    self.own_y().wait_send()
+
+                for way in self.passes:
+                    peer = self.column if way == "column" else self.row
+                    pl.when(self.peer(peer))(lambda: self.relays[way]().wait_send())
 
         def total(at, count):
             out = at(0)[...].astype(f32)
@@ -455,6 +485,7 @@
                     red_w.at[i, : dp_count - 1],
                 ),
                 i,
+                ("column", "row") if z == 1 else (),
             )
             for i in range(hg)
         ]
@@ -470,6 +501,7 @@
                 red_d.at[: dp_count - 1],
             ),
             hg,
+            ("column", "row") if z == 1 else (),
         )
         terms_l = Reduction(
             makes_l,
@@ -483,6 +515,7 @@
                 red_l.at[: dp_count - 1],
             ),
             hg + 1,
+            ("column",),
         )
 
         def vec(at):
@@ -744,13 +777,24 @@
             late_go[1].start()
             late_b[me] = late_s[1]
 
+        def put_sums(h, whole):
+            for i in range(lines):
+                to = slice((h * lines + i) * 128, (h * lines + i + 1) * 128)
+                grad_gain[:, to] = whole[i : i + 1]
+                grad_shift[:, to] = whole[lines + i : lines + i + 1]
+
         def take_early():
             early_go[2].arrive()
-            summed[2 * lines :, :] = total(lambda j: early_b.at[j], 2)
+            whole = total(lambda j: early_b.at[j], 2)
+            put_sums(1, whole)
+            for g in range(groups):
+                for c in range(per_span):
+                    at = 2 * lines + g * per_span + c
+                    grad_bias[g : g + 1, c * 128 : (c + 1) * 128] = whole[at : at + 1]
 
         def take_late():
             late_go[1].arrive()
-            summed[: 2 * lines, :] = total(lambda j: late_b.at[j], spans * QUAD)
+            put_sums(0, total(lambda j: late_b.at[j], spans * QUAD))
 
         go_mix[z].arrive()
         for i, g in enumerate(wide):
@@ -823,21 +867,20 @@
         for term in terms_w:
             term.pass_round()
         if z == 1:
+            give_v()
+        if z == 1:
+            for term in (terms_d, *terms_w):
+                term.relay_column()
             py[hg - 1].start()
-        if z == 1:
-            give_v()
+        terms_l.over_spans()
         spread_early()
         if z == 1:
             spread_late()
-        terms_l.over_spans()
-
-        def relay_terms():
-            for term in (terms_d, *terms_w):
-                term.relay()
 
         for i, g in enumerate(wide):
             if z == 1 and i == hg - 1:
-                relay_terms()
+                for term in (terms_d, *terms_w):
+                    term.relay_row()
                 respread_early()
                 terms_l.pass_round()
             py[i].wait_recv()
@@ -848,11 +891,13 @@
                 give_u(g, whole)
         if z == 0:
             send_late()
+            terms_l.pass_round()
             respread_early()
+            terms_l.relay_column()
             spread_late()
-            terms_l.pass_round()
-            relay_terms()
             give_v()
+        else:
+            terms_l.relay_column()
 
         def put(g, first, block):
             grad_mix[:, g, first * tok : first * tok + block.shape[1]] = block.astype(f32)
@@ -902,7 +947,6 @@
                         put(hg + i, b + 2, all_w[2 + b, i][:, tok:])
 
             term.leave()
-        terms_l.relay()
         terms_l.arrive()
         for t in range(1, QUAD, 2):
 
@@ -922,28 +966,15 @@
         pl.when(zb == z)(functools.partial(run, z))
 
 
-def finish(
-    u_in, v_in, mix_in, summed, grad_u, grad_v, grad_mix, grad_bias, grad_gain, grad_shift, sems
-):
+def finish(*refs):
+    count = len(refs) // 2
+    sems = refs[-1]
     copies = [
         pltpu.make_async_copy(src, dst, sems.at[i])
-        for i, (src, dst) in enumerate(((u_in, grad_u), (v_in, grad_v), (mix_in, grad_mix)))
+        for i, (src, dst) in enumerate(zip(refs[:count], refs[count : 2 * count]))
     ]
     for copy in copies:
         copy.start()
-    groups, span = grad_bias.shape
-    lines = grad_gain.shape[-1] // 2 // 128
-    per_span = span // 128
-    for h in range(2):
-        for i in range(lines):
-            to = slice((h * lines + i) * 128, (h * lines + i + 1) * 128)
-            at = 2 * h * lines + i
-            grad_gain[:, to] = summed[at : at + 1, :]
-            grad_shift[:, to] = summed[lines + at : lines + at + 1, :]
-    for g in range(groups):
-        for c in range(per_span):
-            at = 4 * lines + g * per_span + c
-            grad_bias[g : g + 1, c * 128 : (c + 1) * 128] = summed[at : at + 1, :]
     for copy in copies:
         copy.wait()
 
@@ -1009,19 +1040,22 @@
         + [dma((2, groups)), dma((4, hg)), dma((2, hg))]
         + [dma((4 + hg, dp_count - 1)), dma((2, dp_count - 1)), dma((2 + hg,)), dma((10,))]
         + [dma((2 + hg, spans - 1))] * 2
-        + [dma((2 + hg, 3))] * 2
+        + [dma((2 + hg, 4)), dma((2 + hg, 3))]
         + [dma((7,))]
+    )
+    shapes = (
+        jax.ShapeDtypeStruct((tok, half), bf16),
+        jax.ShapeDtypeStruct((tok, half), bf16),
+        jax.ShapeDtypeStruct((rows, groups, span), f32),
+        jax.ShapeDtypeStruct((1, half), f32),
+        jax.ShapeDtypeStruct((1, half), f32),
+        jax.ShapeDtypeStruct((groups, span), f32),
     )
     out = pl.pallas_call(
         functools.partial(kernel, (tok, width, groups, span, dp_count, spans)),
-        out_shape=(
-            jax.ShapeDtypeStruct((tok, half), bf16),
-            jax.ShapeDtypeStruct((tok, half), bf16),
-            jax.ShapeDtypeStruct((rows, groups, span), f32),
-            jax.ShapeDtypeStruct((late_rows + early_rows, 128), f32),
-        ),
+        out_shape=shapes,
         in_specs=[hbm] * 7,
-        out_specs=[vmem] * 4,
+        out_specs=[vmem] * 6,
         scratch_shapes=scratch,
         compiler_params=pltpu.CompilerParams(
             collective_id=0, has_side_effects=True, vmem_limit_bytes=36 * 1024 * 1024
@@ -1040,19 +1074,12 @@
             )
         )
     )
-    u, v, mix, bias, gain_g, shift_g = pl.pallas_call(
+    u, v, mix, gain_g, shift_g, bias = pl.pallas_call(
         finish,
-        out_shape=(
-            jax.ShapeDtypeStruct((tok, half), bf16),
-            jax.ShapeDtypeStruct((tok, half), bf16),
-            jax.ShapeDtypeStruct((rows, groups, span), f32),
-            jax.ShapeDtypeStruct((groups, span), f32),
-            jax.ShapeDtypeStruct((1, half), f32),
-            jax.ShapeDtypeStruct((1, half), f32),
-        ),
-        in_specs=[vmem] * 4,
-        out_specs=[hbm] * 3 + [vmem] * 3,
-        scratch_shapes=[pltpu.SemaphoreType.DMA((3,))],
+        out_shape=shapes,
+        in_specs=[vmem] * 6,
+        out_specs=[hbm] * 6,
+        scratch_shapes=[dma((6,))],
         compiler_params=pltpu.CompilerParams(vmem_limit_bytes=36 * 1024 * 1024),
     )(*out)
     return (u[None], v[None], mix, bias, gain_g[0], shift_g[0])

time: 46.2 us -> 43.2 us (0.935)
  the two profiles are of different devices: /device:TPU:3 before, /device:TPU:0 now
where the time goes in v3:
time: 43.2 us; the launch traced here: 42.5 us
  Pallas kernels  41.9 us (97%)
  between operations  0.64 us (1%)
    pallas_call x1, Pallas kernels, per_device(): pl.pallas_call(functools.partial(kernel, (tok, width, groups, span, dp_co...  40.4 us
    pallas_call x1, Pallas kernels, per_device(): pl.pallas_call(finish, out_shape=shapes, in_specs=[vmem] * 6, out_specs=[...  1.55 us

profile of v3, /device:TPU:0, one launch (start us, length us, event | category | flops | bytes accessed | tf_op | source)
XLA Modules:
  0.0 42.5 jit_solution(16616682860574836545)
XLA Ops:
  0.6 40.4 %shard_map.118 = (bf16[128,3072]{1,0:T(8,128)(2,1)S(1)}, bf16[128,3072]{1,0:T(8,128)(2,1)S(1)}, f32[128,4,512]{2,1,0:T(4,128)S(1)}, f32[1,3072]{1,0:T(1,128)S(1)...) custom-call(bf16[128,3072]{1,0:T(8,128)(2,1)} %bitcast.9, bf16[128,3072]{1,0:T(8,128)(2,1)} %bitcast.10, ...), custom_call_target="tpu_custom_call" | custom-call | tf_op jit(solution)/shard_map/pallas_call | solution.py:1054
  41.0 1.5 %shard_map.119 = (bf16[128,3072]{1,0:T(8,128)(2,1)}, bf16[128,3072]{1,0:T(8,128)(2,1)}, f32[128,4,512]{2,1,0:T(4,128)}, f32[1,3072]{1,0:T(1,128)}, f32[1,3072]{1,0:T(1,128)}, /*index=5*/f32[4,512]{1,0:T(4,128)}) custom-call(bf16[128,3072]{1,0:T(8,128)(2,1)S(1)} %get-tuple-element.18.refs_0_, bf16[128,3072]{1,0:T(8,128)(2,1)S(1)} %get-tuple-element.19.refs_1_, ...), custom_call_target="tpu_custom_call" | custom-call | tf_op jit(solution)/shard_map/pallas_call | solution.py:1077

commit v4 on v3

--- a/solution.py
+++ b/solution.py
@@ -424,7 +424,7 @@
                     self.to_span.start()
                     over(my_span)[...] = dp_sum[...]
 
-            def pass_round(self):
+            def pass_round(self, along_y=True):
                 red, dp_sum, over, every, _bulk = self.refs
 
                 @pl.when(self.makes(t_own))
@@ -432,7 +432,11 @@
                     self.to_span.arrive()
                     every(k)[...] = total(over, spans).astype(bf16)
                     self.own_z().start()
-                    self.own_y().start()
+                    if along_y:
+                        self.own_y().start()
+
+            def pass_along_y(self):
+                pl.when(self.makes(t_own))(lambda: self.own_y().start())
 
             def relay_column(self):
                 @pl.when(self.peer(self.column))
@@ -863,26 +867,24 @@
         send_early()
         if z == 1:
             send_late()
-        terms_d.pass_round()
-        for term in terms_w:
-            term.pass_round()
-        if z == 1:
-            give_v()
+        for term in (terms_d, *terms_w):
+            term.pass_round(along_y=z == 1)
+        terms_l.over_spans()
         if z == 1:
             for term in (terms_d, *terms_w):
                 term.relay_column()
             py[hg - 1].start()
-        terms_l.over_spans()
         spread_early()
         if z == 1:
             spread_late()
 
         for i, g in enumerate(wide):
             if z == 1 and i == hg - 1:
+                terms_l.pass_round()
                 for term in (terms_d, *terms_w):
                     term.relay_row()
                 respread_early()
-                terms_l.pass_round()
+                give_v()
             py[i].wait_recv()
             whole = own_part[i] + recv_y[i].astype(f32)
             if z == 0:
@@ -891,10 +893,12 @@
                 give_u(g, whole)
         if z == 0:
             send_late()
+            for term in (*terms_w, terms_d):
+                term.pass_along_y()
             terms_l.pass_round()
             respread_early()
+            spread_late()
             terms_l.relay_column()
-            spread_late()
             give_v()
         else:
             terms_l.relay_column()

time: 43.2 us -> 42.5 us (0.984)
  no operation moved by 1% of the time
where the time goes in v4:
time: 42.5 us; the launch traced here: 42.2 us
  Pallas kernels  41.6 us (98%)
  between operations  0.64 us (2%)
    pallas_call x1, Pallas kernels, per_device(): pl.pallas_call(functools.partial(kernel, (tok, width, groups, span, dp_co...  40 us
    pallas_call x1, Pallas kernels, per_device(): pl.pallas_call(finish, out_shape=shapes, in_specs=[vmem] * 6, out_specs=[...  1.55 us

profile of v4, /device:TPU:0, one launch (start us, length us, event | category | flops | bytes accessed | tf_op | source)
XLA Modules:
  0.0 42.2 jit_solution(12647291634452367822)
XLA Ops:
  0.6 40.0 %shard_map.118 = (bf16[128,3072]{1,0:T(8,128)(2,1)S(1)}, bf16[128,3072]{1,0:T(8,128)(2,1)S(1)}, f32[128,4,512]{2,1,0:T(4,128)S(1)}, f32[1,3072]{1,0:T(1,128)S(1)...) custom-call(bf16[128,3072]{1,0:T(8,128)(2,1)} %bitcast.9, bf16[128,3072]{1,0:T(8,128)(2,1)} %bitcast.10, ...), custom_call_target="tpu_custom_call" | custom-call | tf_op jit(solution)/shard_map/pallas_call | solution.py:1058
  40.7 1.5 %shard_map.119 = (bf16[128,3072]{1,0:T(8,128)(2,1)}, bf16[128,3072]{1,0:T(8,128)(2,1)}, f32[128,4,512]{2,1,0:T(4,128)}, f32[1,3072]{1,0:T(1,128)}, f32[1,3072]{1,0:T(1,128)}, /*index=5*/f32[4,512]{1,0:T(4,128)}) custom-call(bf16[128,3072]{1,0:T(8,128)(2,1)S(1)} %get-tuple-element.18.refs_0_, bf16[128,3072]{1,0:T(8,128)(2,1)S(1)} %get-tuple-element.19.refs_1_, ...), custom_call_target="tpu_custom_call" | custom-call | tf_op jit(solution)/shard_map/pallas_call | solution.py:1081

commit v5 on v4

--- a/solution.py
+++ b/solution.py
@@ -529,8 +529,8 @@
             across(
                 lambda j: late_s.at[0],
                 lambda j: late_a.at[j],
+                lambda step: in_sem.at[0],
                 vec(0),
-                vec(1),
                 bulk=late_a.at[: dp_count - 1],
             ),
             Exchange(
@@ -539,8 +539,8 @@
                 me,
                 spans * QUAD,
                 sp_id,
-                vec(2),
-                vec(3),
+                lambda step: in_sem.at[1],
+                vec(1),
                 bulk=late_b.at[: spans * QUAD - 1],
             ),
         )
@@ -548,8 +548,8 @@
             across(
                 lambda j: early_s.at[0],
                 lambda j: early_a.at[j],
-                vec(4),
-                vec(5),
+                lambda step: in_sem.at[2],
+                vec(2),
                 bulk=early_a.at[: dp_count - 1],
             ),
             Exchange(
@@ -558,8 +558,8 @@
                 me // 2,
                 spans * QUAD // 2,
                 lambda j: {"sp": 2 * j + lax.rem(me, 2)},
-                vec(6),
-                vec(7),
+                lambda step: in_sem.at[3],
+                vec(3),
                 bulk=early_c.at[: spans * QUAD // 2 - 1],
             ),
             Exchange(
@@ -568,8 +568,8 @@
                 lax.rem(me, 2),
                 2,
                 lambda j: {"sp": me - lax.rem(me, 2) + j},
-                vec(8),
-                vec(9),
+                lambda step: in_sem.at[4],
+                vec(4),
             ),
         )
 
@@ -577,7 +577,7 @@
             for fetch in (fetches[4], fetches[5], fetches[2]):
                 fetch.wait()
 
-            @pl.loop(0, tok // CHUNK, unroll=4)
+            @pl.loop(0, tok // CHUNK, unroll=8)
             def _(r):
                 at = piece(r)
                 raw = values[at, :].astype(f32)
@@ -933,7 +933,6 @@
                 for i in range(hg):
                     put(i if t >= 2 else hg + i, t, all_d[t, i])
 
-        terms_d.leave()
         for i, term in enumerate(terms_w):
             term.arrive()
             put(i, 0, all_w[lax.rem(t_own, 2), i])
@@ -950,7 +949,6 @@
                     for b in range(t - 1):
                         put(hg + i, b + 2, all_w[2 + b, i][:, tok:])
 
-            term.leave()
         terms_l.arrive()
         for t in range(1, QUAD, 2):
 
@@ -959,12 +957,13 @@
                 for i in range(hg):
                     put(i if t >= 2 else hg + i, t - 1, all_l[t, i])
 
-        terms_l.leave()
         take_early()
         for go in early_go[1:]:
             go.leave()
         take_late()
         late_go[1].leave()
+        for term in (terms_d, *terms_w, terms_l):
+            term.leave()
 
     for z in range(2):
         pl.when(zb == z)(functools.partial(run, z))
@@ -1042,7 +1041,7 @@
             pltpu.VMEM((groups, tok, 128), f32),
         ]
         + [dma((2, groups)), dma((4, hg)), dma((2, hg))]
-        + [dma((4 + hg, dp_count - 1)), dma((2, dp_count - 1)), dma((2 + hg,)), dma((10,))]
+        + [dma((4 + hg, dp_count - 1)), dma((2, dp_count - 1)), dma((2 + hg,)), dma((5,))]
         + [dma((2 + hg, spans - 1))] * 2
         + [dma((2 + hg, 4)), dma((2 + hg, 3))]
         + [dma((7,))]

time: 42.5 us -> 42.5 us (level)
  no operation moved by 1% of the time
where the time goes in v5:
time: 42.5 us; the launch traced here: 42.2 us
  Pallas kernels  41.6 us (98%)
  between operations  0.64 us (2%)
    pallas_call x1, Pallas kernels, per_device(): pl.pallas_call(functools.partial(kernel, (tok, width, groups, span, dp_co...  40 us
    pallas_call x1, Pallas kernels, per_device(): pl.pallas_call(finish, out_shape=shapes, in_specs=[vmem] * 6, out_specs=[...  1.55 us

profile of v5, /device:TPU:0, one launch (start us, length us, event | category | flops | bytes accessed | tf_op | source)
XLA Modules:
  0.0 42.2 jit_solution(2459946773255647691)
XLA Ops:
  0.6 40.0 %shard_map.118 = (bf16[128,3072]{1,0:T(8,128)(2,1)S(1)}, bf16[128,3072]{1,0:T(8,128)(2,1)S(1)}, f32[128,4,512]{2,1,0:T(4,128)S(1)}, f32[1,3072]{1,0:T(1,128)S(1)...) custom-call(bf16[128,3072]{1,0:T(8,128)(2,1)} %bitcast.9, bf16[128,3072]{1,0:T(8,128)(2,1)} %bitcast.10, ...), custom_call_target="tpu_custom_call" | custom-call | tf_op jit(solution)/shard_map/pallas_call | solution.py:1057
  40.7 1.5 %shard_map.119 = (bf16[128,3072]{1,0:T(8,128)(2,1)}, bf16[128,3072]{1,0:T(8,128)(2,1)}, f32[128,4,512]{2,1,0:T(4,128)}, f32[1,3072]{1,0:T(1,128)}, f32[1,3072]{1,0:T(1,128)}, /*index=5*/f32[4,512]{1,0:T(4,128)}) custom-call(bf16[128,3072]{1,0:T(8,128)(2,1)S(1)} %get-tuple-element.18.refs_0_, bf16[128,3072]{1,0:T(8,128)(2,1)S(1)} %get-tuple-element.19.refs_1_, ...), custom_call_target="tpu_custom_call" | custom-call | tf_op jit(solution)/shard_map/pallas_call | solution.py:1080
